TPU v7x, 512 devices: a whole 4x4x16 slice. The times are simulated.
512 devices in a mesh: ep: 32 (over z, core), tp: 16 (over y, x).
Axes of the slice: x: 4, y: 4, z: 16, core: 2. Of those that a mesh axis runs over, the one named last changes fastest.
Arguments:
- recurrence_queries: bfloat16 [16384, 2048], P('ep', 'tp'), may hold values from -6 to 6
- forget_preact: bfloat16 [16384, 2048], P('ep', 'tp')
- recurrence_values: bfloat16 [16384, 2048], P('ep', 'tp'), may hold values from -6 to 6
- output_gate_preact: bfloat16 [16384, 2048], P('ep', 'tp'), may hold values from -6 to 6
- forget_floor_logits: float32 [2048], P('tp')
- surge_log_decay: float32 [16384, 16], P('ep', 'tp'), may hold values from -0.7 to 0
- head_norm_gain: float32 [128], replicated, may hold values from 0.1 to 1.9
- recurrence_out_weight: bfloat16 [2048, 2048], P(None, 'tp'), may hold values from -0.125 to 0.125
- second_micro_rows: bfloat16 [4096, 2048], P('ep'), may hold values from -6 to 6
- expert_norm_gain: float32 [2048], replicated, may hold values from 0.1 to 1.9
- row_group_index: int32 [4096], P('ep'), may hold values from 0 to 3, as said below
- group_expert_index: int32 [4096, 2], P('ep'), may hold values from 0 to 7, as said below
- chosen_expert_weight: float32 [4096, 2], P('ep'), may hold values from 0.2 to 1
- expert_gate_weight: bfloat16 [32, 2048, 4096], P('ep', None, 'tp'), may hold values from -0.125 to 0.125
- expert_up_weight: bfloat16 [32, 2048, 4096], P('ep', None, 'tp'), may hold values from -0.125 to 0.125
- expert_down_weight: bfloat16 [32, 4096, 2048], P('ep', None, 'tp'), may hold values from -0.09375 to 0.09375
Outputs:
- mixed: bfloat16 [16384, 2048], P('ep', 'tp')
- expert_out: bfloat16 [4096, 2048], P('ep', 'tp')
Inputs may be any that keep to these rules, and one draw needn't show every extreme that they name: group_expert_index names two different experts of the row's group; the expert's number is row_group_index * 8 + group_expert_index. Among the rows of one index of ep no expert is named more than 12 times, and some expert exactly 12 times. `group_expert_index`: the two entries of a row differ.
All inputs are finite; a program needn't handle non-finite values.
Results may differ from a plain program's by a relative error of at most 0.009.
Values may be sent and summed in bfloat16 or wider, within the bound.
A program may use at most 64 MiB of HBM per device.

v0:
```python
import jax
import jax.numpy as jnp
from jax import lax
from jax.sharding import Mesh
from jax.sharding import PartitionSpec as P

BLOCK = 64
GROUPS = 4
CAP = 12
EP = ("ep_0", "ep_1")
TP = ("tp_0", "tp_1")


NORM_EPS = 1e-06


def collected_together(array, axis):
    leaves = jax.tree.leaves(array)
    sequence = sorted(range(len(leaves)), key=lambda k: -leaves[k].size)
    width = (1, *leaves[sequence[0]].shape)[-1]
    lines = [
        jnp.pad(leaves[k].reshape(-1), (0, -leaves[k].size % width)).reshape(-1, width)
        for k in sequence
    ]
    both, at, found = (lax.all_gather(jnp.concatenate(lines), axis), 0, {})
    for k, line in zip(sequence, lines):
        piece = both[:, at : at + len(line)].reshape(len(both), -1)
        found[k] = piece[:, : leaves[k].size].reshape(-1, *leaves[k].shape)
        at += len(line)
    numbers = iter(range(len(leaves)))
    return jax.tree.map(lambda _: found[next(numbers)], array)


def entering(array, axis, combine, identity):
    peers, mine = (lax.axis_size(axis), lax.axis_index(axis))
    everything = collected_together(array, axis)
    start = jax.tree.map(
        lambda part, zero: jnp.broadcast_to(jnp.asarray(zero, part.dtype), part.shape),
        array,
        identity,
    )

    def hop(k, before):
        reached = k < mine
        new = combine(before, jax.tree.map(lambda part: part[k], everything))
        return jax.tree.map(lambda a, b: jnp.where(reached, a, b), new, before)

    return lax.fori_loop(0, peers, hop, start)


def joined_along(blocks, dim):
    dims = list(blocks.shape[1:])
    dims[dim] *= blocks.shape[0]
    return jnp.moveaxis(blocks, 0, dim).reshape(dims)


def from_everyone(array, axis):
    peers = lax.axis_size(axis)
    return lax.all_to_all(
        jnp.broadcast_to(array[None], (peers, *array.shape)), axis, 0, 0, tiled=True
    )


def collect(array, axis, dim):
    return joined_along(from_everyone(array, axis), dim)


def cut_along(array, dim, peers):
    before, after = (array.shape[:dim], array.shape[dim + 1 :])
    return jnp.moveaxis(array.reshape(*before, peers, -1, *after), dim, 0)


def moved_by_axis(blocks, axes, sequence):
    inside = blocks.shape[1:]
    out = blocks.reshape(*(lax.axis_size(a) for a in axes), *inside)
    for k in sequence:
        out = lax.all_to_all(out, axes[k], k, k, tiled=True)
    return out.reshape(-1, *inside)


def exchange_by_chip(array, groups, sequence, split_dim, concat_dim):
    peers = lax.axis_size(groups[0]) * lax.axis_size(groups[1])
    blocks = cut_along(array, split_dim, peers)
    return joined_along(moved_by_axis(blocks, groups, sequence), concat_dim)


def whole_of(array, axes, dim):
    out = array
    for number in range(len(axes) - 1, -1, -1):
        out = lax.all_gather(out, axes[number], axis=dim, tiled=True)
    return out


def block_recurrence(query_activated, key_in, value_act, forget_log_value, state_init):
    block_len = query_activated.shape[1]
    causal = (jnp.arange(block_len)[:, None] >= jnp.arange(block_len)[None, :])[:, :, None, None]

    def block_step(current_state, block_inputs):
        query_tile, key_tile, value_tile, g_block = block_inputs
        running_total_sum = jnp.cumsum(g_block, axis=0)
        state_carried_out = jnp.einsum(
            "cra,ran->crn", query_tile * jnp.exp(running_total_sum), current_state
        )
        relative = jnp.where(causal, running_total_sum[:, None] - running_total_sum[None, :], 0.0)
        decays = jnp.where(causal, jnp.exp(relative), 0.0)
        scores = jnp.einsum("thk,tshk,shk->hts", query_tile, decays, key_tile)
        output = state_carried_out + jnp.einsum("hts,shv->thv", scores, value_tile)
        final_log_value = running_total_sum[-1]
        current_state = jnp.exp(final_log_value)[:, :, None] * current_state + jnp.einsum(
            "ceu,cex->eux",
            key_tile * jnp.exp(final_log_value[None] - running_total_sum),
            value_tile,
        )
        return (current_state, output)

    return lax.scan(block_step, state_init, (query_activated, key_in, value_act, forget_log_value))


def carry_join(earlier, later):
    return (earlier[0] * later[0], later[0][:, :, None] * earlier[1] + later[1])


def token_mixing_layer(
    recurrence_queries,
    forget_preact,
    recurrence_values,
    output_gate_preact,
    forget_floor_logits,
    surge_log_decay,
    head_norm_gain,
    recurrence_out_weight,
):
    token_inputs = recurrence_queries.shape[0]
    number_of_heads = surge_log_decay.shape[1]
    key_feature_width = recurrence_queries.shape[1] // number_of_heads
    val_dim = recurrence_values.shape[1] // number_of_heads
    rate = jax.nn.sigmoid(-forget_floor_logits)
    input_gate_value = rate * jax.nn.sigmoid(-forget_preact.astype(jnp.float32))
    forget_log_value = (
        jnp.log1p(-input_gate_value).reshape(token_inputs, number_of_heads, key_feature_width)
        + surge_log_decay[:, :, None]
    )
    query_activated = jax.nn.silu(recurrence_queries.astype(jnp.float32)).reshape(
        token_inputs, number_of_heads, key_feature_width
    )
    key_in = input_gate_value.reshape(token_inputs, number_of_heads, key_feature_width)
    value_act = recurrence_values.astype(jnp.float32).reshape(
        token_inputs, number_of_heads, val_dim
    )
    block_count = token_inputs // BLOCK

    def to_blocks(array):
        return array.reshape(block_count, BLOCK, number_of_heads, array.shape[-1])

    state_init = jnp.zeros((number_of_heads, key_feature_width, val_dim), jnp.float32)
    ending, recur_out = block_recurrence(
        to_blocks(query_activated),
        to_blocks(key_in),
        to_blocks(value_act),
        to_blocks(forget_log_value),
        state_init,
    )
    recur_out = recur_out.reshape(token_inputs, number_of_heads, val_dim)
    total_decay = jnp.exp(jnp.sum(forget_log_value, axis=0))
    incoming_state = entering(
        (total_decay, ending), EP, carry_join, (jnp.ones_like(total_decay), jnp.zeros_like(ending))
    )[1]
    running_state = jnp.cumsum(forget_log_value, axis=0)
    recur_out = recur_out + jnp.einsum(
        "cra,ran->crn", query_activated * jnp.exp(running_state), incoming_state
    )
    normed = (
        recur_out
        * lax.rsqrt(jnp.mean(recur_out * recur_out, axis=-1, keepdims=True) + NORM_EPS)
        * head_norm_gain
    )
    gate_act = jax.nn.silu(output_gate_preact.astype(jnp.float32)).reshape(
        token_inputs, number_of_heads, val_dim
    )
    gated_heads = (
        (normed * gate_act).reshape(token_inputs, number_of_heads * val_dim).astype(jnp.bfloat16)
    )
    return jnp.dot(
        collect(gated_heads, TP, 1), recurrence_out_weight, preferred_element_type=jnp.float32
    ).astype(jnp.bfloat16)


def routed_experts(
    second_micro_rows,
    expert_norm_gain,
    row_group_index,
    group_expert_index,
    chosen_expert_weight,
    expert_gate_weight,
    expert_up_weight,
    expert_down_weight,
):
    row_count = second_micro_rows.shape[0]
    model_width = second_micro_rows.shape[1]
    columns = model_width // lax.axis_size(TP)
    local_count = expert_gate_weight.shape[0]
    expert_count = local_count * lax.axis_size(EP)
    per_group = expert_count // GROUPS
    rows_float = second_micro_rows.astype(jnp.float32)
    normed_rows = (
        rows_float
        * lax.rsqrt(jnp.mean(rows_float * rows_float, axis=-1, keepdims=True) + NORM_EPS)
        * expert_norm_gain
    ).astype(jnp.bfloat16)
    flat_expert = (row_group_index[:, None] * per_group + group_expert_index).reshape(-1)
    onehot = (flat_expert[:, None] == jnp.arange(expert_count, dtype=jnp.int32)[None, :]).astype(
        jnp.int32
    )
    rank_index = jnp.sum((jnp.cumsum(onehot, axis=0) - onehot) * onehot, axis=1)
    slot_index = flat_expert * CAP + rank_index
    owner_row = (
        jnp.full((expert_count * CAP,), row_count, jnp.int32)
        .at[slot_index]
        .set(jnp.arange(2 * row_count) // 2)
    )
    col_part = lax.dynamic_slice_in_dim(normed_rows, lax.axis_index(TP) * columns, columns, 1)
    padded = jnp.concatenate([col_part, jnp.zeros((1, columns), jnp.bfloat16)], axis=0)
    outgoing = padded[owner_row].reshape(expert_count, CAP, columns)
    arrived = exchange_by_chip(outgoing, ("ep_0", "ep_1"), (1, 0), 0, 1)
    arrived = collect(arrived, TP, 2)
    gate_act = jnp.einsum(
        "erd,edf->erf", arrived, expert_gate_weight, preferred_element_type=jnp.float32
    )
    up_act = jnp.einsum(
        "erd,edf->erf", arrived, expert_up_weight, preferred_element_type=jnp.float32
    )
    hidden = (jax.nn.silu(gate_act) * up_act).astype(jnp.bfloat16)
    result = jnp.einsum(
        "erf,efd->erd",
        whole_of(hidden, TP, 2),
        expert_down_weight,
        preferred_element_type=jnp.float32,
    ).astype(jnp.bfloat16)
    returned = lax.all_to_all(result, EP, split_axis=1, concat_axis=0, tiled=True)
    picked = returned.reshape(expert_count * CAP, expert_down_weight.shape[2])[slot_index]
    picked = picked.reshape(row_count, 2, expert_down_weight.shape[2]).astype(jnp.float32)
    return jnp.sum(picked * chosen_expert_weight[:, :, None], axis=1).astype(jnp.bfloat16)


def local(
    recurrence_queries,
    forget_preact,
    recurrence_values,
    output_gate_preact,
    forget_floor_logits,
    surge_log_decay,
    head_norm_gain,
    recurrence_out_weight,
    second_micro_rows,
    expert_norm_gain,
    row_group_index,
    group_expert_index,
    chosen_expert_weight,
    expert_gate_weight,
    expert_up_weight,
    expert_down_weight,
):
    mixed = token_mixing_layer(
        recurrence_queries,
        forget_preact,
        recurrence_values,
        output_gate_preact,
        forget_floor_logits,
        surge_log_decay,
        head_norm_gain,
        recurrence_out_weight,
    )
    expert_out = routed_experts(
        second_micro_rows,
        expert_norm_gain,
        row_group_index,
        group_expert_index,
        chosen_expert_weight,
        expert_gate_weight,
        expert_up_weight,
        expert_down_weight,
    )
    return (mixed, expert_out)


def solution(mesh):
    finer = Mesh(mesh.devices.reshape(16, 2, 4, 4), ("ep_0", "ep_1", "tp_0", "tp_1"))
    in_specs = (
        P(EP, TP),
        P(EP, TP),
        P(EP, TP),
        P(EP, TP),
        P(TP),
        P(EP, TP),
        P(),
        P(None, TP),
        P(EP, None),
        P(),
        P(EP),
        P(EP, None),
        P(EP, None),
        P(EP, None, TP),
        P(EP, None, TP),
        P(EP, None, TP),
    )
    out_specs = (P(EP, TP), P(EP, TP))
    return jax.shard_map(local, mesh=finer, in_specs=in_specs, out_specs=out_specs, check_vma=False)
```

profile of v0, /device:TPU:1, one launch (start us, length us, event | category | flops | bytes accessed | tf_op | source)
XLA Modules:
  0.0 210.5 jit_solution(1780213694522339451)
XLA Ops:
  7.3 1.1 copy.76
  9.0 1.0 fusion.68
  10.2 1.0 copy.79
  11.9 12.5 %while.29 = (s32[]{:T(128)}, f32[1,128,128]{2,1,0:T(8,128)S(1)}, f32[8,64,1,128]{3,1,2,0:T(8,128)S(1)}, f32[8,64,1,128]{3,1,2,0:T(8,128)S(1)}, f32[8,64,1,128]{3...) while((s32[]{:T(128)}, f32[1,128,128]{2,1,0:T(8,128)S(1)}, ...), condition=%wide.region_2.3_spmd.clone.clone, body=%wide.region_0.2_spmd.clone.clone.sunk | while | flops 9007107 | bytes 978044 | solution.py:116
  12.1 0.9 fusion.116
  13.7 0.9 fusion.116
  15.3 0.9 fusion.116
  16.8 0.9 fusion.116
  18.4 0.9 fusion.116
  20.0 0.9 fusion.116
  21.5 0.9 fusion.116
  23.1 0.9 fusion.116
  28.0 1.4 scatter_custom_fusion
  29.4 1.4 gather_fusion
  30.9 10.3 %all_to_all.29 = bf16[16,2,1,12,128]{4,0,3,2,1:T(8,128)(2,1)S(1)} all-to-all(bf16[16,2,1,12,128]{4,0,3,2,1:T(8,128)(2,1)S(1)} %copy.94), channel_id=1, replica_groups=mesh['ep_0'=16,'ep_1'=2,'tp_0'=4,'tp_1'=4] {'ep_1'}, dimensions={1} | all-to-all | bytes 196608 | tf_op jit(solution)/shard_map/all_to_all | solution.py:77
  41.3 21.2 %all_to_all.30 = bf16[16,2,1,12,128]{4,1,3,2,0:T(2,128)(2,1)S(1)} all-to-all(bf16[16,2,1,12,128]{4,1,3,2,0:T(2,128)(2,1)S(1)} %copy.95), channel_id=1, replica_groups=mesh['ep_0'=16,'ep_1'=2,'tp_0'=4,'tp_1'=4] {'ep_0'}, dimensions={0} | all-to-all | bytes 196608 | tf_op jit(solution)/shard_map/all_to_all | solution.py:77
  62.7 1.4 broadcast_in_dim.71
  64.0 6.7 %all-to-all-start.3 = ((bf16[16,1,384,128]{2,3,1,0:T(8,128)(2,1)}), bf16[16,1,384,128]{2,3,1,0:T(8,128)(2,1)S(1)}, u32[]{:S(2)}, u32[]{:S(2)}) async-start(bf16[16,1,384,128]{2,3,1,0:T(8,128)(2,1)} %broadcast_in_dim.71), calls=%async_computation.3 | async-start | bytes 3145728 | tf_op jit(solution)/shard_map/all_to_all | solution.py:59
  74.2 1.0 copy.89
  75.2 15.1 %all-to-all-done.3 = bf16[16,1,384,128]{2,3,1,0:T(8,128)(2,1)S(1)} async-done(((bf16[16,1,384,128]{2,3,1,0:T(8,128)(2,1)}), bf16[16,1,384,128]{2,3,1,0:T(8,128)(2,1)S(1)}, u32[]{:S(2)}, u32[]{:S(2)}) %all-to-all-start.3) | async-done | bytes 1572896 | tf_op jit(solution)/shard_map/all_to_all | solution.py:59
  92.1 12.4 %all-gather.1 = bf16[384,1024]{1,0:T(8,128)(2,1)} all-gather(bf16[384,256]{1,0:T(8,128)(2,1)S(1)} %fusion.36), channel_id=3, replica_groups=mesh['ep_0'=16,'ep_1'=2,'tp_0'=4,'tp_1'=4] {'tp_1'}, dimensions={1}, use_global_device_ids=true | all-gather | bytes 983040 | tf_op jit(solution)/shard_map/all_gather | solution.py:90
  104.6 1.8 slice_bitcast_fusion.1
  107.3 4.2 %while.28 = (s32[]{:T(128)}, f32[1,128,128]{2,1,0:T(8,128)S(1)}, s32[]{:T(128)}, f32[32,1,128]{2,1,0:T(1,128)S(1)}, f32[32,1,128,128]{3,2,1,0:T(8,128)S(1)}, /*index=5*/s32[]{:T(128)}, s32[]{:T(128)}) while((s32[]{:T(128)}, f32[1,128,128]{2,1,0:T(8,128)S(1)}, s32[]{:T(128)}, f32[32,1,128]{2,1,0:T(1,128)S(1)}, ...), condition=%wide.region_5.6_spmd.clone, body=%wide.region_4.5_spmd.clone.sunk | while | flops 65540 | bytes 198249 | solution.py:48
  111.6 1.4 multiply_reduce_fusion.1
  113.1 1.6 broadcast_in_dim.67
  114.7 5.9 %all-to-all-start = ((bf16[16,512,128]{1,2,0:T(8,128)(2,1)}), bf16[16,512,128]{1,2,0:T(8,128)(2,1)S(1)}, u32[]{:S(2)}, u32[]{:S(2)}) async-start(bf16[16,512,128]{1,2,0:T(8,128)(2,1)} %broadcast_in_dim.67), calls=%async_computation | async-start | bytes 4194304 | tf_op jit(solution)/shard_map/all_to_all | solution.py:59
  120.7 52.0 %all-gather.7.cloned.1.call-done = bf16[384,4096]{1,0:T(8,128)(2,1)} async-done(((bf16[384,1024]{1,0:T(8,128)(2,1)}), bf16[384,4096]{1,0:T(8,128)(2,1)}) %all-gather.7.cloned.1.call-update) | async-done | bytes 3145744 | tf_op jit(solution)/shard_map/all_gather | solution.py:90
  172.7 3.1 %fusion.38 = bf16[1,384,128]{2,1,0:T(8,128)(2,1)S(1)} fusion(bf16[384,4096]{1,0:T(8,128)(2,1)} %all-gather.7.cloned.1.call-done, bf16[1,4096,128]{2,1,0:T(8,128)(2,1)} %param.35), kind=kOutput, calls=%fused_computation.56 | convolution fusion | flops 402702336 | bytes 4292608 | tf_op jit(solution)/shard_map/erf,efd->erd/dot_general | solution.py:233
  176.5 1.2 reduce.5
  178.4 8.7 %all-to-all-start.4 = ((bf16[32,2,768]{2,1,0:T(2,128)(2,1)}), bf16[32,2,768]{2,1,0:T(2,128)(2,1)S(1)}, u32[]{:S(2)}, u32[]{:S(2)}) async-start(bf16[32,2,768]{2,1,0:T(2,128)(2,1)} %reshape.427), calls=%async_computation.4 | async-start | bytes 196608 | tf_op jit(solution)/shard_map/all_to_all | solution.py:239
  187.1 2.5 %convolution_convert_fusion = bf16[512,128]{1,0:T(8,128)(2,1)} fusion(bf16[512,2048]{0,1:T(8,128)(2,1)S(1)} %bitcast.240, bf16[2048,128]{1,0:T(8,128)(2,1)} %param.27), kind=kOutput, calls=%fused_computation.54 | convolution fusion | flops 268500992 | bytes 2752512 | tf_op jit(solution)/shard_map/dot_general | solution.py:183
  189.6 12.3 %all-to-all-done.4 = bf16[32,2,768]{2,1,0:T(2,128)(2,1)S(1)} async-done(((bf16[32,2,768]{2,1,0:T(2,128)(2,1)}), bf16[32,2,768]{2,1,0:T(2,128)(2,1)S(1)}, u32[]{:S(2)}, u32[]{:S(2)}) %all-to-all-start.4) | async-done | bytes 98336 | tf_op jit(solution)/shard_map/all_to_all | solution.py:239
  (236 shorter events, 22.7 us)
Async XLA Ops:
  7.2 83.1 %copy-start = (bf16[1,2048,256]{2,1,0:T(8,128)(2,1)S(1)}, bf16[1,2048,256]{2,1,0:T(8,128)(2,1)}, u32[]{:S(2)}) copy-start(bf16[1,2048,256]{2,1,0:T(8,128)(2,1)} %param.33) | copy-start | bytes 3145732
  7.2 4.3 %copy-start.4 = (bf16[512,128]{1,0:T(8,128)(2,1)S(1)}, bf16[512,128]{1,0:T(8,128)(2,1)}, u32[]{:S(2)}) copy-start(bf16[512,128]{1,0:T(8,128)(2,1)} %param.22) | copy-start | bytes 393220
  7.2 97.4 %all-gather.9.cloned.1.call-start = ((), (), s32[]{:S(2)}) async-start(), calls=%async_computation.6 | async-start | bytes 2297856 | tf_op jit(solution)/shard_map/all_gather | solution.py:25
  11.2 0.7 copy-start.2
  11.9 13.2 %copy-start.9 = (s32[128]{0:T(128)S(1)}, s32[128]{0:T(128)}, u32[]{:S(2)}) copy-start(s32[128]{0:T(128)} %param.30) | copy-start | bytes 1540
  11.9 13.2 %copy-start.6 = (s32[128,2]{0,1:T(2,128)S(1)}, s32[128,2]{0,1:T(2,128)}, u32[]{:S(2)}) copy-start(s32[128,2]{0,1:T(2,128)} %param.31) | copy-start | bytes 3076
  11.9 13.6 %copy-start.1 = (bf16[128,2048]{1,0:T(8,128)(2,1)S(1)}, bf16[128,2048]{1,0:T(8,128)(2,1)}, u32[]{:S(2)}) copy-start(bf16[128,2048]{1,0:T(8,128)(2,1)} %param.28) | copy-start | bytes 1572868
  64.0 26.2 %all-to-all-start.3 = ((bf16[16,1,384,128]{2,3,1,0:T(8,128)(2,1)}), bf16[16,1,384,128]{2,3,1,0:T(8,128)(2,1)S(1)}, u32[]{:S(2)}, u32[]{:S(2)}) async-start(bf16[16,1,384,128]{2,3,1,0:T(8,128)(2,1)} %broadcast_in_dim.71), calls=%async_computation.3 | async-start | bytes 3145728 | tf_op jit(solution)/shard_map/all_to_all | solution.py:59
  70.8 101.9 %all-gather.7.cloned.1.call-start = ((), (), s32[]{:S(2)}) async-start(), calls=%async_computation.5 | async-start | bytes 3932160 | tf_op jit(solution)/shard_map/all_gather | solution.py:90
  90.3 1.2 copy-start.8
  104.6 7.0 %copy-start.3 = (bf16[512,128]{0,1:T(8,128)(2,1)S(1)}, bf16[512,128]{0,1:T(8,128)(2,1)}, u32[]{:S(2)}) copy-start(bf16[512,128]{0,1:T(8,128)(2,1)} %copy-done.2) | copy-start | bytes 393220
  106.4 6.6 %copy-start.7 = (f32[128]{0:T(128)S(1)}, f32[128]{0:T(128)}, u32[]{:S(2)}) copy-start(f32[128]{0:T(128)} %param.26) | copy-start | bytes 1540
  114.7 5.9 %copy-start.5 = (f32[128,2]{0,1:T(2,128)S(1)}, f32[128,2]{0,1:T(2,128)}, u32[]{:S(2)}) copy-start(f32[128,2]{0,1:T(2,128)} %param.32) | copy-start | bytes 3076
  114.7 63.7 %all-to-all-start = ((bf16[16,512,128]{1,2,0:T(8,128)(2,1)}), bf16[16,512,128]{1,2,0:T(8,128)(2,1)S(1)}, u32[]{:S(2)}, u32[]{:S(2)}) async-start(bf16[16,512,128]{1,2,0:T(8,128)(2,1)} %broadcast_in_dim.67), calls=%async_computation | async-start | bytes 4194304 | tf_op jit(solution)/shard_map/all_to_all | solution.py:59
  178.4 23.4 %all-to-all-start.4 = ((bf16[32,2,768]{2,1,0:T(2,128)(2,1)}), bf16[32,2,768]{2,1,0:T(2,128)(2,1)S(1)}, u32[]{:S(2)}, u32[]{:S(2)}) async-start(bf16[32,2,768]{2,1,0:T(2,128)(2,1)} %reshape.427), calls=%async_computation.4 | async-start | bytes 196608 | tf_op jit(solution)/shard_map/all_to_all | solution.py:239
Sparse Core Ops, SparseCore 0:
  25.2 78.5 all-gather.8
  106.0 66.7 all-gather.6
where the time goes:
time: 211 us; the launch traced here: 210 us
  waiting for transfers between devices  79.4 us (38%)
  blocking collectives  43.9 us (21%)
  starting transfers between devices  21.4 us (10%)
  local copies, waits for them, and re-layouts  20.9 us (10%)
  matrix products  19.5 us (9%)
  between operations  14.6 us (7%)
  other arithmetic  9.43 us (4%)
    all_gather x1, waiting for transfers between devices, whole_of(): out = lax.all_gather(out, axes[number], axis=dim, tiled=True)  52 us
    all_to_all x2, blocking collectives, moved_by_axis(): out = lax.all_to_all(out, axes[k], k, k, tiled=True)  31.5 us
    all_to_all x2, waiting for transfers between devices, from_everyone(): lax.all_to_all(jnp.broadcast_to(array[None], (peers, *array.shape)), axis...  15.1 us
    all_to_all x2, starting transfers between devices, from_everyone(): lax.all_to_all(jnp.broadcast_to(array[None], (peers, *array.shape)), axis...  12.7 us
    all_gather x1, blocking collectives, whole_of(): out = lax.all_gather(out, axes[number], axis=dim, tiled=True)  12.4 us
    all_to_all x1, waiting for transfers between devices, routed_experts(): lax.all_to_all(result, EP, split_axis=1, concat_axis=0, tiled=True)  12.3 us
    all_to_all x1, starting transfers between devices, routed_experts(): lax.all_to_all(result, EP, split_axis=1, concat_axis=0, tiled=True)  8.66 us
    dot_general x8, matrix products, block_step(): scores = jnp.einsum('thk,tshk,shk->hts', query_tile, decays, key_tile)  7.51 us
  transfers between devices with their start and end apart: 5, of which 3 were waited for; matrix products, arithmetic and copies ran while one was open for 14% of the time, Pallas kernels for 0%

commit v1 on v0

v1 whole, which is shorter than its diff:
```python
import functools

import jax
import jax.numpy as jnp
from jax import lax
from jax.experimental import pallas as pl
from jax.experimental.pallas import tpu as pltpu
from jax.sharding import PartitionSpec as P

MESH = pl.DeviceIdType.MESH
F32, BF16 = jnp.float32, jnp.bfloat16
EPS = 1e-06
GROUPS = 4
CAP = 12
SLOT = 16
SIDE = 4
NT = (((1,), (1,)), ((), ()))
OFFSETS = (0, -1, 1, 2)


def silu(v):
    return v / (1.0 + jnp.exp(-v))


class Gather:
    def __init__(self, buf, send, recv, ep, y, x):
        self.buf, self.send, self.recv, self.ep, self.y, self.x = buf, send, recv, ep, y, x
        self.rows = buf.shape[1]

    def tp(self, color, a, b):
        dy, dx = (b, a) if color == 0 else (a, b)
        return lax.rem(self.y + dy + SIDE, SIDE) * SIDE + lax.rem(self.x + dx + SIDE, SIDE)

    def span(self, color, part):
        half = self.rows // 2
        start = color * half
        if part == 1:
            return pl.ds(start, half // 2)
        if part == 2:
            return pl.ds(start + half // 2, half // 2)
        return pl.ds(start, half)

    def copy(self, color, slot, block, part, to):
        region = self.buf.at[self.tp(color, *block), self.span(color, part), :]
        return pltpu.make_async_remote_copy(
            src_ref=region,
            dst_ref=region,
            send_sem=self.send.at[color, slot],
            recv_sem=self.recv.at[color, slot],
            device_id=(self.ep, self.tp(color, *to)),
            device_id_type=MESH,
        )

    def out(self, slot):
        if slot < 4:
            return [((0, 0), 0, (1, 0)), ((0, 0), 0, (-1, 0)), ((-1, 0), 1, (1, 0)), ((1, 0), 2, (-1, 0))][slot]
        j, k = divmod(slot - 4, 4)
        a = OFFSETS[j]
        return [((a, 0), 0, (0, 1)), ((a, 0), 0, (0, -1)), ((a, -1), 1, (0, 1)), ((a, 1), 2, (0, -1))][k]

    def landed(self, slot):
        if slot < 4:
            return [((-1, 0), 0), ((1, 0), 0), ((2, 0), 1), ((2, 0), 2)][slot]
        j, k = divmod(slot - 4, 4)
        a = OFFSETS[j]
        return [((a, -1), 0), ((a, 1), 0), ((a, 2), 1), ((a, 2), 2)][k]

    def start(self, color, *slots):
        for slot in slots:
            self.copy(color, slot, *self.out(slot)).start()

    def arrive(self, color, *slots):
        for slot in slots:
            block, part = self.landed(slot)
            self.copy(color, slot, block, part, (1, 0)).wait_recv()

    def begin(self):
        for color in (0, 1):
            self.start(color, 0, 1, 4, 5)

    def relay(self):
        for k in (0, 1):
            for color in (0, 1):
                self.arrive(color, k)
                self.start(color, 2 + k, 4 + 4 * (k + 1), 5 + 4 * (k + 1))
        for color in (0, 1):
            self.arrive(color, 4)
            self.start(color, 6)
            self.arrive(color, 5)
            self.start(color, 7)
        for color in (0, 1):
            self.arrive(color, 2, 3)
            self.start(color, 16, 17)
        for j in (1, 2, 3):
            for color in (0, 1):
                self.arrive(color, 4 + 4 * j)
                self.start(color, 6 + 4 * j)
                self.arrive(color, 5 + 4 * j)
                self.start(color, 7 + 4 * j)
        for j in (0, 1, 2, 3):
            for color in (0, 1):
                self.arrive(color, 6 + 4 * j, 7 + 4 * j)

    def drain(self):
        for color in (0, 1):
            for slot in range(20):
                self.copy(color, slot, *self.out(slot)).wait_send()


def exchange_copy(src, dst, send, recv, peer, mine, tp):
    return pltpu.make_async_remote_copy(
        src_ref=src,
        dst_ref=dst,
        send_sem=send.at[peer],
        recv_sem=recv.at[mine],
        device_id=(peer, tp),
        device_id_type=MESH,
    )


def kernel(
    n_ep,
    q_hbm, fp_hbm, v_hbm, og_hbm, floor_ref, surge_ref, gain_ref, wout_hbm,
    rows_hbm, ngain_ref, grp_ref, gex_ref, cw_ref, wg_hbm, wu_hbm, wd_hbm,
    mixed_ref, eout_ref,
    q_b, fp_b, v_b, og_b, rows_b, wout_b, wg_b, wu_b, wd_b, in_sem,
    outgo, arrived, result, returned, weights,
    xbuf, hbuf, mbuf,
    cum, keyin, qact, qdec, local_out,
    state, slices, decays, own_decay, prefix, incoming,
    d_send, d_recv, c_send, c_recv,
    s_send, s_recv, e_send, e_recv, p_send, p_recv,
    x_send, x_recv, h_send, h_recv, m_send, m_recv,
):
    me, tp = lax.axis_index("ep"), lax.axis_index("tp")
    y, x = lax.div(tp, SIDE), lax.rem(tp, SIDE)
    n_serve = n_ep // 2
    serving = lax.rem(me, 2) == 1
    share = lax.div(me, 2)

    barrier = pltpu.get_barrier_semaphore()

    @pl.loop(1, n_ep)
    def _(d):
        pl.semaphore_signal(barrier, inc=1, device_id=(lax.rem(me + d, n_ep), tp), device_id_type=MESH)

    for dy, dx in ((0, 1), (0, -1), (1, 0), (-1, 0)):
        other = lax.rem(y + dy + SIDE, SIDE) * SIDE + lax.rem(x + dx + SIDE, SIDE)
        pl.semaphore_signal(barrier, inc=1, device_id=(me, other), device_id_type=MESH)

    loads = {}
    for k, (name, src, dst) in enumerate(
        (
            ("rows", rows_hbm, rows_b), ("fp", fp_hbm, fp_b), ("q", q_hbm, q_b), ("v", v_hbm, v_b),
            ("og", og_hbm, og_b), ("wg", wg_hbm.at[0], wg_b), ("wu", wu_hbm.at[0], wu_b),
            ("wd", wd_hbm.at[0], wd_b), ("wout", wout_hbm, wout_b),
        )
    ):
        loads[name] = pltpu.make_async_copy(src, dst, in_sem.at[k])
        loads[name].start()

    count = grp_ref.shape[1]
    per_group = n_ep // GROUPS
    ex0 = grp_ref[...] * per_group + gex_ref[0:1, :]
    ex1 = grp_ref[...] * per_group + gex_ref[1:2, :]
    e_iota = lax.broadcasted_iota(jnp.int32, (n_ep, count), 0)
    hit0, hit1 = (e_iota == ex0).astype(F32), (e_iota == ex1).astype(F32)
    before = lax.broadcasted_iota(jnp.int32, (count, count), 0) < lax.broadcasted_iota(jnp.int32, (count, count), 1)
    earlier = jnp.dot((hit0 + hit1).astype(BF16), before.astype(F32).astype(BF16), preferred_element_type=F32)
    slot0 = ex0 * SLOT + jnp.sum(earlier * hit0, axis=0, keepdims=True).astype(jnp.int32)
    slot1 = ex1 * SLOT + jnp.sum(earlier * hit1, axis=0, keepdims=True).astype(jnp.int32)
    s_iota = lax.broadcasted_iota(jnp.int32, (n_ep * SLOT, count), 0)
    at0, at1 = s_iota == slot0, s_iota == slot1
    chosen = jnp.where(at0, cw_ref[0:1, :], 0.0) + jnp.where(at1, cw_ref[1:2, :], 0.0)
    turned = chosen.T
    high = turned.astype(BF16)
    weights[0] = high
    weights[1] = (turned - high.astype(F32)).astype(BF16)
    place = jnp.where(at0 | at1, 1.0, 0.0).astype(BF16)

    loads["rows"].wait()
    columns = pl.ds(pl.multiple_of(tp * 128, 128), 128)
    square = jnp.zeros((count, 128), F32)
    for k in range(rows_b.shape[1] // 128):
        part = rows_b[:, k * 128 : (k + 1) * 128].astype(F32)
        square = square + part * part
    scale = lax.rsqrt(jnp.sum(square, axis=1, keepdims=True) * (1.0 / rows_b.shape[1]) + EPS)
    normed = (rows_b[:, columns].astype(F32) * scale * ngain_ref[:, columns]).astype(BF16)
    outgo[...] = jnp.dot(place, normed, preferred_element_type=F32).astype(BF16).reshape(outgo.shape)

    pl.semaphore_wait(barrier, n_ep - 1 + 4)

    @pl.loop(1, n_ep)
    def _(d):
        peer = lax.rem(me + d, n_ep)
        exchange_copy(outgo.at[peer], arrived.at[me], d_send, d_recv, peer, me, tp).start()

    loads["fp"].wait()
    loads["q"].wait()
    loads["v"].wait()
    length = fp_b.shape[0]
    rate = jax.nn.sigmoid(-floor_ref[...])
    lower = lax.broadcasted_iota(jnp.int32, (128, 128), 0) >= lax.broadcasted_iota(jnp.int32, (128, 128), 1)
    lower = jnp.where(lower, 1.0, 0.0)
    carry = jnp.zeros((1, 128), F32)
    for b in range(length // 128):
        r = slice(b * 128, b * 128 + 128)
        gate = rate * jax.nn.sigmoid(-fp_b[r, :].astype(F32))
        keyin[r, :] = gate
        total = jnp.dot(lower, jnp.log1p(-gate), precision=lax.Precision.HIGHEST, preferred_element_type=F32)
        total = total + jnp.sum(lower * surge_ref[b : b + 1, :], axis=1, keepdims=True) + carry
        cum[r, :] = total
        carry = total[127:128, :]
        qact[r, :] = silu(q_b[r, :].astype(F32))

    own_decay[0] = jnp.exp(carry)
    tail = jnp.exp(carry - cum[...]) * keyin[...]
    state[...] = jnp.dot(v_b[...].astype(F32).T.astype(BF16), tail.astype(BF16), preferred_element_type=F32).reshape(
        state.shape
    )

    @pl.loop(0, n_serve)
    def _(k):
        peer = 2 * k + 1

        @pl.when(peer != me)
        def _():
            exchange_copy(state.at[k], slices.at[me], s_send, s_recv, peer, me, tp).start()
            exchange_copy(own_decay.at[0], decays.at[me], e_send, e_recv, peer, me, tp).start()

    qdec[...] = (qact[...] * jnp.exp(cum[...])).astype(BF16)
    sub = 64

    @pl.loop(0, length // sub)
    def _(c):
        r = pl.ds(pl.multiple_of(c * sub, sub), sub)
        shape = (sub // 8, 8, 128)
        g, k, v = cum[r, :].reshape(shape), keyin[r, :].reshape(shape), v_b[r, :].astype(F32).reshape(shape)
        q = qact[r, :].reshape(shape)
        within = lax.broadcasted_iota(jnp.int32, (sub // 8, 8, 1), 1)
        total = jnp.sum(q * k, axis=2, keepdims=True) * v
        for d in range(1, 8):
            gd, kd, vd = (pltpu.roll(a, d, 1) for a in (g, k, v))
            w = jnp.sum(q * kd * jnp.exp(jnp.minimum(g - gd, 0.0)), axis=2, keepdims=True)
            total = total + jnp.where(within >= d, w, 0.0) * vd
        local_out[r, :] = total.reshape(sub, 128)

    half = length // 2
    t_iota = lax.broadcasted_iota(jnp.int32, (half, half), 0)
    u_iota = lax.broadcasted_iota(jnp.int32, (half, half), 1)
    for b in range(2):
        r = slice(b * half, (b + 1) * half)
        acc = jnp.zeros((half, half), F32)
        h = 8
        while h < half:
            g3 = cum[r, :].reshape(half // (2 * h), 2 * h, 128)
            fade = jnp.exp(-jnp.abs(g3 - g3[:, h - 1 : h, :])).reshape(half, 128)
            s = lax.dot_general(
                (qact[r, :] * fade).astype(BF16), (keyin[r, :] * fade).astype(BF16), NT, preferred_element_type=F32
            )
            pair = (t_iota // (2 * h) == u_iota // (2 * h)) & ((t_iota // h) % 2 == 1) & ((u_iota // h) % 2 == 0)
            acc = jnp.where(pair, s, acc)
            h *= 2
        local_out[r, :] += jnp.dot(acc.astype(BF16), v_b[r, :], preferred_element_type=F32)
    edge = cum[half - 1 : half, :]
    left, right = slice(0, half), slice(half, length)
    s = lax.dot_general(
        (qact[right, :] * jnp.exp(cum[right, :] - edge)).astype(BF16),
        (keyin[left, :] * jnp.exp(edge - cum[left, :])).astype(BF16),
        NT,
        preferred_element_type=F32,
    )
    local_out[right, :] += jnp.dot(s.astype(BF16), v_b[left, :], preferred_element_type=F32)

    @pl.when(serving)
    def _():
        slices[me] = state[share]
        decays[me] = own_decay[0]

        @pl.loop(1, n_ep)
        def _(d):
            peer = lax.rem(me + d, n_ep)
            exchange_copy(state.at[0], slices.at[peer], s_send, s_recv, me, peer, tp).wait_recv()
            exchange_copy(own_decay.at[0], decays.at[peer], e_send, e_recv, me, peer, tp).wait_recv()

        total = jnp.zeros(slices.shape[1:], F32)
        for k in range(n_ep):
            prefix[k] = total
            total = decays[k] * total + slices[k]

        @pl.loop(1, n_ep)
        def _(d):
            peer = lax.rem(me + d, n_ep)
            exchange_copy(prefix.at[peer], incoming.at[share], p_send, p_recv, peer, share, tp).start()

        incoming[share] = prefix[me]

    arrived[me] = outgo[me]

    @pl.loop(1, n_ep)
    def _(d):
        peer = lax.rem(me + d, n_ep)
        exchange_copy(outgo.at[peer], arrived.at[peer], d_send, d_recv, me, peer, tp).wait_recv()

    exp_rows = n_ep * CAP
    row = lax.broadcasted_iota(jnp.int32, (exp_rows, n_ep * SLOT), 0)
    col = lax.broadcasted_iota(jnp.int32, (exp_rows, n_ep * SLOT), 1)
    pack = jnp.where(row // CAP * SLOT + row % CAP == col, 1.0, 0.0).astype(BF16)
    xbuf[tp] = jnp.dot(pack, arrived[...].reshape(n_ep * SLOT, 128), preferred_element_type=F32).astype(BF16)
    gather_x = Gather(xbuf, x_send, x_recv, me, y, x)
    gather_h = Gather(hbuf, h_send, h_recv, me, y, x)
    gather_m = Gather(mbuf, m_send, m_recv, me, y, x)
    gather_x.begin()

    @pl.loop(0, n_serve)
    def _(k):
        @pl.when(2 * k + 1 != me)
        def _():
            exchange_copy(prefix.at[0], incoming.at[k], p_send, p_recv, me, k, tp).wait_recv()

    before_state = incoming[...].reshape(128, 128).astype(BF16)
    loads["og"].wait()
    out = local_out[...] + lax.dot_general(qdec[...], before_state, NT, preferred_element_type=F32)
    out = out * lax.rsqrt(jnp.mean(out * out, axis=1, keepdims=True) + EPS) * gain_ref[...]
    mbuf[tp] = (out * silu(og_b[...].astype(F32))).astype(BF16)

    gather_x.relay()
    loads["wg"].wait()
    loads["wu"].wait()
    tps = SIDE * SIDE
    feats = jnp.concatenate([xbuf[k] for k in range(tps)], axis=1)
    gate_act = jnp.dot(feats, wg_b[...], preferred_element_type=F32)
    up_act = jnp.dot(feats, wu_b[...], preferred_element_type=F32)
    hbuf[tp] = (silu(gate_act) * up_act).astype(BF16)
    gather_h.begin()
    gather_h.relay()
    gather_m.begin()
    loads["wd"].wait()
    hidden = jnp.concatenate([hbuf[k] for k in range(tps)], axis=1)
    res = jnp.dot(hidden, wd_b[...], preferred_element_type=F32).astype(BF16)
    row = lax.broadcasted_iota(jnp.int32, (n_ep * SLOT, exp_rows), 0)
    col = lax.broadcasted_iota(jnp.int32, (n_ep * SLOT, exp_rows), 1)
    spread = jnp.where((row // SLOT * CAP + row % SLOT == col) & (row % SLOT < CAP), 1.0, 0.0).astype(BF16)
    result[...] = jnp.dot(spread, res, preferred_element_type=F32).astype(BF16).reshape(result.shape)

    @pl.loop(1, n_ep)
    def _(d):
        peer = lax.rem(me + d, n_ep)
        exchange_copy(result.at[peer], returned.at[me], c_send, c_recv, peer, me, tp).start()

    returned[me] = result[me]
    gather_m.relay()
    loads["wout"].wait()
    heads = jnp.concatenate([mbuf[k] for k in range(tps)], axis=1)
    mixed_ref[...] = jnp.dot(heads, wout_b[...], preferred_element_type=F32).astype(BF16)

    @pl.loop(1, n_ep)
    def _(d):
        peer = lax.rem(me + d, n_ep)
        exchange_copy(result.at[peer], returned.at[peer], c_send, c_recv, me, peer, tp).wait_recv()

    back = returned[...].reshape(n_ep * SLOT, 128)
    eout_ref[...] = (
        jnp.dot(weights[0], back, preferred_element_type=F32) + jnp.dot(weights[1], back, preferred_element_type=F32)
    ).astype(BF16)

    @pl.loop(1, n_ep)
    def _(d):
        peer = lax.rem(me + d, n_ep)
        exchange_copy(outgo.at[peer], arrived.at[me], d_send, d_recv, peer, me, tp).wait_send()
        exchange_copy(result.at[peer], returned.at[me], c_send, c_recv, peer, me, tp).wait_send()

        @pl.when(serving)
        def _():
            exchange_copy(prefix.at[peer], incoming.at[share], p_send, p_recv, peer, share, tp).wait_send()

    @pl.loop(0, n_serve)
    def _(k):
        peer = 2 * k + 1

        @pl.when(peer != me)
        def _():
            exchange_copy(state.at[k], slices.at[me], s_send, s_recv, peer, me, tp).wait_send()
            exchange_copy(own_decay.at[0], decays.at[me], e_send, e_recv, peer, me, tp).wait_send()

    for gather in (gather_x, gather_h, gather_m):
        gather.drain()


def solution(mesh):
    n_ep, n_tp = mesh.shape["ep"], mesh.shape["tp"]

    def local(q, fp, v, og, floor, surge, gain, wout, rows, ngain, grp, gex, cw, wg, wu, wd):
        length, count = q.shape[0], rows.shape[0]
        hid, cols = wg.shape[2], wd.shape[2]
        exp_rows = n_ep * CAP
        vmem, anyspace = pl.BlockSpec(memory_space=pltpu.VMEM), pl.BlockSpec(memory_space=pl.ANY)
        dma = pltpu.SemaphoreType.DMA
        block = (n_ep, SLOT, 128)
        scratch = [
            pltpu.VMEM(q.shape, BF16), pltpu.VMEM(q.shape, BF16), pltpu.VMEM(q.shape, BF16), pltpu.VMEM(q.shape, BF16),
            pltpu.VMEM(rows.shape, BF16), pltpu.VMEM(wout.shape, BF16),
            pltpu.VMEM(wg.shape[1:], BF16), pltpu.VMEM(wu.shape[1:], BF16), pltpu.VMEM(wd.shape[1:], BF16),
            dma((9,)),
            pltpu.VMEM(block, BF16), pltpu.VMEM(block, BF16), pltpu.VMEM(block, BF16), pltpu.VMEM(block, BF16),
            pltpu.VMEM((2, count, n_ep * SLOT), BF16),
            pltpu.VMEM((n_tp, exp_rows, 128), BF16), pltpu.VMEM((n_tp, exp_rows, hid), BF16),
            pltpu.VMEM((n_tp, length, 128), BF16),
            pltpu.VMEM(q.shape, F32), pltpu.VMEM(q.shape, F32), pltpu.VMEM(q.shape, F32), pltpu.VMEM(q.shape, BF16),
            pltpu.VMEM(q.shape, F32),
            pltpu.VMEM((n_ep // 2, 256 // n_ep, 128), F32), pltpu.VMEM((n_ep, 256 // n_ep, 128), F32),
            pltpu.VMEM((n_ep, 1, 128), F32), pltpu.VMEM((1, 1, 128), F32),
            pltpu.VMEM((n_ep, 256 // n_ep, 128), F32), pltpu.VMEM((n_ep // 2, 256 // n_ep, 128), F32),
            dma((n_ep,)), dma((n_ep,)), dma((n_ep,)), dma((n_ep,)),
            dma((n_ep,)), dma((n_ep,)), dma((n_ep,)), dma((n_ep,)), dma((n_ep,)), dma((n_ep,)),
            dma((2, 20)), dma((2, 20)), dma((2, 20)), dma((2, 20)), dma((2, 20)), dma((2, 20)),
        ]
        return pl.pallas_call(
            functools.partial(kernel, n_ep),
            out_shape=(jax.ShapeDtypeStruct((length, cols), BF16), jax.ShapeDtypeStruct((count, cols), BF16)),
            in_specs=[anyspace] * 4 + [vmem] * 3 + [anyspace] * 2 + [vmem] * 4 + [anyspace] * 3,
            out_specs=(vmem, vmem),
            scratch_shapes=scratch,
            compiler_params=pltpu.CompilerParams(
                collective_id=0, has_side_effects=True, vmem_limit_bytes=60 * 1024 * 1024
            ),
        )(
            q, fp, v, og, floor.reshape(1, -1), surge.reshape(-1, 128), gain.reshape(1, -1), wout,
            rows, ngain.reshape(1, -1), grp.reshape(1, -1), gex.T, cw.T, wg, wu, wd,
        )

    return jax.shard_map(
        local,
        mesh=mesh,
        in_specs=(
            P("ep", "tp"), P("ep", "tp"), P("ep", "tp"), P("ep", "tp"), P("tp"), P("ep", "tp"), P(), P(None, "tp"),
            P("ep", None), P(), P("ep"), P("ep", None), P("ep", None),
            P("ep", None, "tp"), P("ep", None, "tp"), P("ep", None, "tp"),
        ),
        out_specs=(P("ep", "tp"), P("ep", "tp")),
        check_vma=False,
    )
```

time: 211 us -> 101 us (0.48)
  the two profiles are of different devices: /device:TPU:1 before, /device:TPU:2 now
where the time goes in v1:
time: 101 us
  Pallas kernels  98.1 us (97%)
  local copies, waits for them, and re-layouts  2.19 us (2%)
    pallas_call x1, Pallas kernels, local(): pl.pallas_call(functools.partial(kernel, n_ep), out_shape=(jax.ShapeDtype...  98.1 us
    unnamed x4, local copies, waits for them, and re-layouts  2.19 us

profile of v1, /device:TPU:2, one launch (start us, length us, event | category | flops | bytes accessed | tf_op | source)
XLA Modules:
  0.0 100.9 jit_solution(9153658835414533527)
XLA Ops:
  0.6 98.1 %shard_map.167 = (bf16[512,128]{1,0:T(8,128)(2,1)}, bf16[128,128]{1,0:T(8,128)(2,1)}) custom-call(bf16[512,128]{1,0:T(8,128)(2,1)} %q_hbm.1, bf16[512,128]{1,0:T(8,128)(2,1)} %fp_hbm.1, bf16[512,128]{1,0:T(8,128)(2,1)} %v_hbm.1, bf16[512,128]{1,0:T(8,128)(2,1)} %og_hbm.1, f32[1,128]{1,0:T(1,128)} %bitcast.11, f32[4,128]{1,0:T(4,128)} %bitcast.8, ...), custom_call_target="tpu_custom_call" | custom-call | tf_op jit(solution)/shard_map/pallas_call | solution.py:418
  98.7 0.0 copy-start
  98.7 1.6 %copy.20 = bf16[512,128]{1,0:T(8,128)(2,1)} copy(bf16[512,128]{1,0:T(8,128)(2,1)} %get-tuple-element.4) | data formatting | bytes 262144
  100.3 0.0 copy-done
  100.3 0.6 copy.21
Async XLA Ops:
  98.7 1.6 %copy-start = (bf16[128,128]{1,0:T(8,128)(2,1)S(1)}, bf16[128,128]{1,0:T(8,128)(2,1)}, u32[]{:S(2)}) copy-start(bf16[128,128]{1,0:T(8,128)(2,1)} %get-tuple-element.5) | copy-start | bytes 98308

commit v2 on v1

v2 whole, which is shorter than its diff:
```python
import functools

import jax
import jax.numpy as jnp
from jax import lax
from jax.experimental import pallas as pl
from jax.experimental.pallas import tpu as pltpu
from jax.sharding import PartitionSpec as P

MESH = pl.DeviceIdType.MESH
F32, BF16 = jnp.float32, jnp.bfloat16
EPS = 1e-06
GROUPS = 4
CAP = 12
SLOT = 16
SIDE = 4
NT = (((1,), (1,)), ((), ()))
OFFSETS = (0, -1, 1, 2)


def silu(v):
    return v / (1.0 + jnp.exp(-v))


class Gather:
    def __init__(self, buf, base, rows, send, recv, ep, y, x):
        self.buf, self.base, self.rows = buf, base, rows
        self.send, self.recv, self.ep, self.y, self.x = send, recv, ep, y, x

    def tp(self, color, a, b):
        dy, dx = (b, a) if color == 0 else (a, b)
        return lax.rem(self.y + dy + SIDE, SIDE) * SIDE + lax.rem(self.x + dx + SIDE, SIDE)

    def span(self, color, part):
        half = self.rows // 2
        start = self.base + color * half
        if part == 1:
            return pl.ds(start, half // 2)
        if part == 2:
            return pl.ds(start + half // 2, half // 2)
        return pl.ds(start, half)

    def copy(self, color, slot, block, part, to):
        region = self.buf.at[self.tp(color, *block), self.span(color, part), :]
        return pltpu.make_async_remote_copy(
            src_ref=region,
            dst_ref=region,
            send_sem=self.send.at[color, slot],
            recv_sem=self.recv.at[color, slot],
            device_id=(self.ep, self.tp(color, *to)),
            device_id_type=MESH,
        )

    def out(self, slot):
        if slot < 4:
            return [((0, 0), 0, (1, 0)), ((0, 0), 0, (-1, 0)), ((-1, 0), 1, (1, 0)), ((1, 0), 2, (-1, 0))][slot]
        j, k = divmod(slot - 4, 4)
        a = OFFSETS[j]
        return [((a, 0), 0, (0, 1)), ((a, 0), 0, (0, -1)), ((a, -1), 1, (0, 1)), ((a, 1), 2, (0, -1))][k]

    def landed(self, slot):
        if slot < 4:
            return [((-1, 0), 0), ((1, 0), 0), ((2, 0), 1), ((2, 0), 2)][slot]
        j, k = divmod(slot - 4, 4)
        a = OFFSETS[j]
        return [((a, -1), 0), ((a, 1), 0), ((a, 2), 1), ((a, 2), 2)][k]

    def start(self, color, *slots):
        for slot in slots:
            self.copy(color, slot, *self.out(slot)).start()

    def arrive(self, color, *slots):
        for slot in slots:
            block, part = self.landed(slot)
            self.copy(color, slot, block, part, (1, 0)).wait_recv()

    def begin(self):
        for color in (0, 1):
            self.start(color, 0, 1, 4, 5)

    def relay(self):
        self.relay_sends()
        self.relay_last()

    def relay_sends(self):
        self.relay_near()
        self.relay_far()

    def relay_near(self):
        self.relay_first()
        self.relay_second()

    def relay_first(self):
        for k in (0, 1):
            for color in (0, 1):
                self.arrive(color, k)
                self.start(color, 2 + k, 4 + 4 * (k + 1), 5 + 4 * (k + 1))

    def relay_second(self):
        for color in (0, 1):
            self.arrive(color, 4)
            self.start(color, 6)
            self.arrive(color, 5)
            self.start(color, 7)

    def relay_far(self):
        for color in (0, 1):
            self.arrive(color, 2, 3)
            self.start(color, 16, 17)
        for j in (1, 2, 3):
            for color in (0, 1):
                self.arrive(color, 4 + 4 * j)
                self.start(color, 6 + 4 * j)
                self.arrive(color, 5 + 4 * j)
                self.start(color, 7 + 4 * j)

    def relay_last(self):
        for j in (0, 1, 2, 3):
            for color in (0, 1):
                self.arrive(color, 6 + 4 * j, 7 + 4 * j)

    def drain(self):
        for color in (0, 1):
            for slot in range(20):
                self.copy(color, slot, *self.out(slot)).wait_send()


class Ring:
    def __init__(self, turn, send, recv, ep, y, x):
        self.turn, self.send, self.recv, self.ep, self.y, self.x = turn, send, recv, ep, y, x

    def pos(self, half, off=0):
        return lax.rem((self.x if half == self.turn else self.y) + off + SIDE, SIDE)

    def tp(self, half, off):
        if half == self.turn:
            return self.y * SIDE + self.pos(half, off)
        return self.pos(half, off) * SIDE + self.x

    def copy(self, half, slot, src, dst, off):
        return pltpu.make_async_remote_copy(
            src_ref=src,
            dst_ref=dst,
            send_sem=self.send.at[half, slot],
            recv_sem=self.recv.at[half, slot],
            device_id=(self.ep, self.tp(half, off)),
            device_id_type=MESH,
        )


def exchange_copy(src, dst, send, recv, peer, mine, tp):
    return pltpu.make_async_remote_copy(
        src_ref=src,
        dst_ref=dst,
        send_sem=send.at[peer],
        recv_sem=recv.at[mine],
        device_id=(peer, tp),
        device_id_type=MESH,
    )


def kernel(
    n_ep,
    q_hbm, fp_hbm, v_hbm, og_hbm, floor_hbm, surge_hbm, gain_hbm, wout_hbm,
    rows_hbm, ngain_hbm, grp_hbm, gex_hbm, cw_hbm, wg_hbm, wu_hbm, wd_hbm,
    mixed_hbm, eout_hbm,
    q_b, fp_b, v_b, og_b, floor_b, surge_b, gain_b, wout_b,
    rows_b, ngain_b, grp_b, gex_b, cw_b, wg_b, wu_b, wd_b, mixed_b, eout_b, in_sem, out_sem, own_sem,
    outgo, arrived, result, returned, weights, pack, spread,
    xbuf, hbuf, mbuf, wcross, staged, part, sums_out, sums_in,
    cum, keyin, qact, qdec, local_out,
    state, slices, decays, own_decay, prefix, incoming,
    d_send, d_recv, c_send, c_recv,
    s_send, s_recv, e_send, e_recv, p_send, p_recv,
    x_send, x_recv, h_send, h_recv, m_send, m_recv, w_send, w_recv, r_send, r_recv,
):
    me, tp = lax.axis_index("ep"), lax.axis_index("tp")
    y, x = lax.div(tp, SIDE), lax.rem(tp, SIDE)
    z, core = lax.div(me, 2), lax.rem(me, 2)
    n_z = n_ep // 2
    serving = core == 1

    loads = {}

    def load(*names):
        for name in names:
            loads[name].start()

    for k, (name, src, dst) in enumerate(
        (
            ("grp", grp_hbm, grp_b), ("gex", gex_hbm, gex_b), ("rows", rows_hbm, rows_b), ("ngain", ngain_hbm, ngain_b),
            ("wd", wd_hbm, wd_b), ("cw", cw_hbm, cw_b), ("floor", floor_hbm, floor_b), ("fp", fp_hbm, fp_b),
            ("surge", surge_hbm, surge_b), ("q", q_hbm, q_b), ("v", v_hbm, v_b), ("og", og_hbm, og_b),
            ("gain", gain_hbm, gain_b), ("wg", wg_hbm.at[0], wg_b), ("wu", wu_hbm.at[0], wu_b), ("wout", wout_hbm, wout_b),
        )
    ):
        loads[name] = pltpu.make_async_copy(src, dst, in_sem.at[k])
    load("grp", "gex", "rows", "ngain")

    barrier = pltpu.get_barrier_semaphore()
    for d in range(1, n_ep):
        pl.semaphore_signal(barrier, inc=1, device_id=(lax.rem(me + d, n_ep), tp), device_id_type=MESH)

    for dy, dx in ((0, 1), (0, -1), (1, 0), (-1, 0)):
        other = lax.rem(y + dy + SIDE, SIDE) * SIDE + lax.rem(x + dx + SIDE, SIDE)
        pl.semaphore_signal(barrier, inc=1, device_id=(me, other), device_id_type=MESH)

    load("wd", "floor", "fp", "surge", "q", "v", "cw", "og", "gain", "wg", "wu", "wout")

    loads["grp"].wait()
    loads["gex"].wait()
    count = grp_b.shape[1]
    per_group = n_ep // GROUPS
    ex0 = grp_b[...] * per_group + gex_b[0:1, :]
    ex1 = grp_b[...] * per_group + gex_b[1:2, :]
    e_iota = lax.broadcasted_iota(jnp.int32, (n_ep, count), 0)
    hit0, hit1 = (e_iota == ex0).astype(F32), (e_iota == ex1).astype(F32)
    before = lax.broadcasted_iota(jnp.int32, (count, count), 0) < lax.broadcasted_iota(jnp.int32, (count, count), 1)
    earlier = jnp.dot((hit0 + hit1).astype(BF16), before.astype(F32).astype(BF16), preferred_element_type=F32)
    slot0 = ex0 * SLOT + jnp.sum(earlier * hit0, axis=0, keepdims=True).astype(jnp.int32)
    slot1 = ex1 * SLOT + jnp.sum(earlier * hit1, axis=0, keepdims=True).astype(jnp.int32)
    s_iota = lax.broadcasted_iota(jnp.int32, (n_ep * SLOT, count), 0)
    at0, at1 = s_iota == slot0, s_iota == slot1
    place = jnp.where(at0 | at1, 1.0, 0.0).astype(BF16)

    loads["rows"].wait()
    loads["ngain"].wait()
    columns = pl.ds(pl.multiple_of(tp * 128, 128), 128)
    square = jnp.zeros((count, 128), F32)
    for k in range(rows_b.shape[1] // 128):
        piece = rows_b[:, k * 128 : (k + 1) * 128].astype(F32)
        square = square + piece * piece
    scale = lax.rsqrt(jnp.sum(square, axis=1, keepdims=True) * (1.0 / rows_b.shape[1]) + EPS)
    normed = (rows_b[:, columns].astype(F32) * scale * ngain_b[:, columns]).astype(BF16)
    outgo[...] = jnp.dot(place, normed, preferred_element_type=F32).astype(BF16).reshape(outgo.shape)

    pl.semaphore_wait(barrier, n_ep - 1 + 4)

    order = [(n_z // 2, c) for c in (1, 0)]
    for away in range(n_z // 2 - 1, 0, -1):
        order += [(way * away, c) for c in (1, 0) for way in (1, -1)]
    order.append((0, 0))
    peers = [lax.rem(z + away + n_z, n_z) * 2 + lax.rem(core + c + 1, 2) for away, c in order]

    def dispatch(peer):
        return exchange_copy(outgo.at[peer], arrived.at[me], d_send, d_recv, peer, me, tp)

    def give_back(peer):
        return exchange_copy(result.at[peer], returned.at[me], c_send, c_recv, peer, me, tp)

    for peer in peers:
        dispatch(peer).start()

    loads["wd"].wait()
    ring_g = Ring(0, h_send, h_recv, me, y, x)
    ring_w = Ring(1, w_send, w_recv, me, y, x)
    ring_r = Ring(1, r_send, r_recv, me, y, x)

    def cross(half, slot):
        mine = ring_w.pos(half)

        def to(off, part):
            there = ring_w.pos(half, off)
            return wd_b.at[there, part] if half == 0 else wd_b.at[part, there]

        whole, low, high = pl.ds(0, SIDE), pl.ds(0, SIDE // 2), pl.ds(SIDE // 2, SIDE // 2)
        src, dst = (
            (lambda: to(2, low), lambda: staged.at[half, 0]),
            (lambda: to(2, high), lambda: staged.at[half, 1]),
            (lambda: to(1, whole), lambda: wcross.at[half, mine]),
            (lambda: to(-1, whole), lambda: wcross.at[half, mine]),
            (lambda: staged.at[half, 0], lambda: wcross.at[half, ring_w.pos(half, -1), low]),
            (lambda: staged.at[half, 1], lambda: wcross.at[half, ring_w.pos(half, 1), high]),
        )[slot]
        return ring_w.copy(half, slot, src(), dst(), (1, -1)[slot % 2])

    def crossed(half, slot):
        low, high = pl.ds(0, SIDE // 2), pl.ds(SIDE // 2, SIDE // 2)
        region = (
            lambda: staged.at[half, 0],
            lambda: staged.at[half, 1],
            lambda: wcross.at[half, ring_w.pos(half, -1)],
            lambda: wcross.at[half, ring_w.pos(half, 1)],
            lambda: wcross.at[half, ring_w.pos(half, 2), low],
            lambda: wcross.at[half, ring_w.pos(half, 2), high],
        )[slot]()
        return ring_w.copy(half, slot, region, region, 1)

    for slot in range(4):
        for half in (0, 1):
            cross(half, slot).start()
    own_w = [
        pltpu.make_async_copy(wd_b.at[y], wcross.at[0, y], own_sem.at[0]),
        pltpu.make_async_copy(wd_b.at[:, x], wcross.at[1, x], own_sem.at[1]),
    ]
    for copy in own_w:
        copy.start()

    loads["floor"].wait()
    loads["fp"].wait()
    loads["surge"].wait()
    loads["q"].wait()
    loads["v"].wait()
    length = fp_b.shape[0]
    rate = jax.nn.sigmoid(-floor_b[...])
    lower = lax.broadcasted_iota(jnp.int32, (128, 128), 0) >= lax.broadcasted_iota(jnp.int32, (128, 128), 1)
    lower = jnp.where(lower, 1.0, 0.0)
    carry = jnp.zeros((1, 128), F32)
    for b in range(length // 128):
        r = slice(b * 128, b * 128 + 128)
        gate = rate * jax.nn.sigmoid(-fp_b[r, :].astype(F32))
        keyin[r, :] = gate
        total = jnp.dot(lower, jnp.log1p(-gate), precision=lax.Precision.HIGHEST, preferred_element_type=F32)
        total = total + jnp.sum(lower * surge_b[b : b + 1, :], axis=1, keepdims=True) + carry
        cum[r, :] = total
        carry = total[127:128, :]
        qact[r, :] = silu(q_b[r, :].astype(F32))

    own_decay[0] = jnp.exp(carry)
    tail = jnp.exp(carry - cum[...]) * keyin[...]
    state[...] = jnp.dot(v_b[...].astype(F32).T.astype(BF16), tail.astype(BF16), preferred_element_type=F32).reshape(
        state.shape
    )

    @pl.loop(0, n_z)
    def _(k):
        peer = 2 * k + 1

        @pl.when(peer != me)
        def _():
            exchange_copy(state.at[k], slices.at[me], s_send, s_recv, peer, me, tp).start()
            exchange_copy(own_decay.at[0], decays.at[me], e_send, e_recv, peer, me, tp).start()

    qdec[...] = (qact[...] * jnp.exp(cum[...])).astype(BF16)
    sub = 64

    @pl.loop(0, length // sub)
    def _(c):
        r = pl.ds(pl.multiple_of(c * sub, sub), sub)
        shape = (sub // 8, 8, 128)
        g, k, v = cum[r, :].reshape(shape), keyin[r, :].reshape(shape), v_b[r, :].astype(F32).reshape(shape)
        q = qact[r, :].reshape(shape)
        within = lax.broadcasted_iota(jnp.int32, (sub // 8, 8, 1), 1)
        total = jnp.sum(q * k, axis=2, keepdims=True) * v
        for d in range(1, 8):
            gd, kd, vd = (pltpu.roll(a, d, 1) for a in (g, k, v))
            w = jnp.sum(q * kd * jnp.exp(jnp.minimum(g - gd, 0.0)), axis=2, keepdims=True)
            total = total + jnp.where(within >= d, w, 0.0) * vd
        local_out[r, :] = total.reshape(sub, 128)

    half = length // 2
    t_iota = lax.broadcasted_iota(jnp.int32, (half, half), 0)
    u_iota = lax.broadcasted_iota(jnp.int32, (half, half), 1)
    for b in range(2):
        r = slice(b * half, (b + 1) * half)
        acc = jnp.zeros((half, half), F32)
        h = 8
        while h < half:
            g3 = cum[r, :].reshape(half // (2 * h), 2 * h, 128)
            fade = jnp.exp(-jnp.abs(g3 - g3[:, h - 1 : h, :])).reshape(half, 128)
            s = lax.dot_general(
                (qact[r, :] * fade).astype(BF16), (keyin[r, :] * fade).astype(BF16), NT, preferred_element_type=F32
            )
            pair = (t_iota // (2 * h) == u_iota // (2 * h)) & ((t_iota // h) % 2 == 1) & ((u_iota // h) % 2 == 0)
            acc = jnp.where(pair, s, acc)
            h *= 2
        local_out[r, :] += jnp.dot(acc.astype(BF16), v_b[r, :], preferred_element_type=F32)
    edge = cum[half - 1 : half, :]
    left, right = slice(0, half), slice(half, length)
    s = lax.dot_general(
        (qact[right, :] * jnp.exp(cum[right, :] - edge)).astype(BF16),
        (keyin[left, :] * jnp.exp(edge - cum[left, :])).astype(BF16),
        NT,
        preferred_element_type=F32,
    )
    local_out[right, :] += jnp.dot(s.astype(BF16), v_b[left, :], preferred_element_type=F32)

    part_rows, part_slots = n_z * CAP, n_z * SLOT

    def matches(shape, axis):
        r, s = lax.broadcasted_iota(jnp.int32, shape, axis), lax.broadcasted_iota(jnp.int32, shape, 1 - axis)
        return jnp.where(r // CAP * SLOT + r % CAP == s, 1.0, 0.0).astype(BF16)

    pack[...] = matches((part_rows, part_slots), 0)
    spread[...] = matches((part_slots, part_rows), 1)
    loads["cw"].wait()
    chosen = jnp.where(at0, cw_b[0:1, :], 0.0) + jnp.where(at1, cw_b[1:2, :], 0.0)
    turned = chosen.T
    high = turned.astype(BF16)
    weights[0] = high
    weights[1] = (turned - high.astype(F32)).astype(BF16)

    gather_x = Gather(xbuf, 0, 2 * part_rows, x_send, x_recv, me, y, x)
    gather_m = Gather(mbuf, 0, length, m_send, m_recv, me, y, x)
    tps = SIDE * SIDE

    for slot in (0, 1):
        for half in (0, 1):
            crossed(half, slot).wait_recv()
            cross(half, slot + 4).start()
    arrived[me] = outgo[me]

    @pl.loop(1, n_ep)
    def _(d):
        peer = lax.rem(me + d, n_ep)
        exchange_copy(outgo.at[0], arrived.at[peer], d_send, d_recv, me, peer, tp).wait_recv()

    for c in range(2):
        blocks = arrived[c * n_z : (c + 1) * n_z].reshape(part_slots, 128)
        xbuf[tp, c * part_rows : (c + 1) * part_rows, :] = jnp.dot(
            pack[...], blocks, preferred_element_type=F32
        ).astype(BF16)
    gather_x.begin()

    gather_x.relay_near()
    @pl.when(serving)
    def _():
        slices[me] = state[z]
        decays[me] = own_decay[0]

        @pl.loop(1, n_ep)
        def _(d):
            peer = lax.rem(me + d, n_ep)
            exchange_copy(state.at[0], slices.at[peer], s_send, s_recv, me, peer, tp).wait_recv()
            exchange_copy(own_decay.at[0], decays.at[peer], e_send, e_recv, me, peer, tp).wait_recv()

        total = jnp.zeros(slices.shape[1:], F32)
        for k in range(n_ep):
            prefix[k] = total
            total = decays[k] * total + slices[k]

        @pl.loop(1, n_ep)
        def _(d):
            peer = lax.rem(me + d, n_ep)
            exchange_copy(prefix.at[peer], incoming.at[z], p_send, p_recv, peer, z, tp).start()

        incoming[z] = prefix[me]

    gather_x.relay_far()
    gather_x.relay_last()
    loads["wg"].wait()
    loads["wu"].wait()
    feats = jnp.concatenate([xbuf[k] for k in range(tps)], axis=1)
    gate_act = jnp.dot(feats, wg_b[...], preferred_element_type=F32)
    up_act = jnp.dot(feats, wu_b[...], preferred_element_type=F32)
    hidden = (silu(gate_act) * up_act).astype(BF16)
    for c in range(2):
        hbuf[c, ring_g.pos(c)] = hidden[c * part_rows : (c + 1) * part_rows, :]

    first, last = pl.ds(0, part_rows // 2), pl.ds(part_rows // 2, part_rows // 2)

    def along(c, slot):
        block = hbuf.at[c, ring_g.pos(c, (0, 0, -1, 1)[slot])]
        block = block if slot < 2 else block.at[first if slot == 2 else last]
        return ring_g.copy(c, slot, block, block, (1, -1, 1, -1)[slot])

    def came_along(c, slot):
        block = hbuf.at[c, ring_g.pos(c, (-1, 1, 2, 2)[slot])]
        block = block if slot < 2 else block.at[first if slot == 2 else last]
        return ring_g.copy(c, slot, block, block, 1)

    for slot in (0, 1):
        for c in (0, 1):
            along(c, slot).start()
    for slot in (0, 1):
        for c in (0, 1):
            came_along(c, slot).wait_recv()
            along(c, slot + 2).start()

    @pl.loop(0, n_z)
    def _(k):
        @pl.when(2 * k + 1 != me)
        def _():
            exchange_copy(prefix.at[0], incoming.at[k], p_send, p_recv, me, k, tp).wait_recv()

    before_state = incoming[...].reshape(128, 128).astype(BF16)
    loads["og"].wait()
    loads["gain"].wait()
    out = local_out[...] + lax.dot_general(qdec[...], before_state, NT, preferred_element_type=F32)
    out = out * lax.rsqrt(jnp.mean(out * out, axis=1, keepdims=True) + EPS) * gain_b[...]
    mbuf[tp] = (out * silu(og_b[...].astype(F32))).astype(BF16)
    gather_m.begin()

    for copy in own_w:
        copy.wait()
    for slot in (2, 3, 4, 5):
        for c in (0, 1):
            crossed(c, slot).wait_recv()
    for slot in (2, 3):
        for c in (0, 1):
            came_along(c, slot).wait_recv()

    sums = ((2, first, 1), (2, last, -1), (1, last, 1), (-1, first, -1), (1, first, 1), (-1, last, -1))

    def across(c, slot):
        target, rows, way = sums[slot]
        return ring_r.copy(c, slot, sums_out.at[c, slot], sums_in.at[c, slot], way)

    for c in (0, 1):
        units = jnp.concatenate([hbuf[c, k] for k in range(SIDE)], axis=1)
        feats = jnp.concatenate([wcross[c, k].reshape(units.shape[1], 128) for k in range(SIDE)], axis=1)
        total = jnp.dot(units, feats, preferred_element_type=F32)
        for k in range(SIDE):
            part[c, k] = total[:, k * 128 : (k + 1) * 128]
        for slot in range(4):
            target, rows, _ = sums[slot]
            sums_out[c, slot] = part[c, ring_r.pos(c, target), rows, :].astype(BF16)
            across(c, slot).start()
    for slot in (0, 1):
        for c in (0, 1):
            across(c, slot).wait_recv()
            target, rows, _ = sums[slot + 4]
            sums_out[c, slot + 4] = (
                part[c, ring_r.pos(c, target), rows, :] + sums_in[c, slot].astype(F32)
            ).astype(BF16)
            across(c, slot + 4).start()
    gather_m.relay_first()
    for c in (0, 1):
        for slot in (2, 3, 4, 5):
            across(c, slot).wait_recv()
        mine = ring_r.pos(c)
        top = part[c, mine, first, :] + sums_in[c, 4].astype(F32) + sums_in[c, 3].astype(F32)
        low = part[c, mine, last, :] + sums_in[c, 2].astype(F32) + sums_in[c, 5].astype(F32)
        res = jnp.concatenate([top, low], axis=0).astype(BF16)
        result[c * n_z : (c + 1) * n_z] = (
            jnp.dot(spread[...], res, preferred_element_type=F32).astype(BF16).reshape(n_z, SLOT, 128)
        )

    for peer in peers:
        give_back(peer).start()

    returned[me] = result[me]
    gather_m.relay_second()
    gather_m.relay_far()
    gather_m.relay_last()
    loads["wout"].wait()
    heads = jnp.concatenate([mbuf[k] for k in range(tps)], axis=1)
    mixed_b[...] = jnp.dot(heads, wout_b[...], preferred_element_type=F32).astype(BF16)
    mixed_out = pltpu.make_async_copy(mixed_b, mixed_hbm, out_sem.at[0])
    mixed_out.start()

    for peer in peers:
        dispatch(peer).wait_send()
        give_back(peer).wait_send()

    @pl.when(serving)
    def _():
        @pl.loop(1, n_ep)
        def _(d):
            peer = lax.rem(me + d, n_ep)
            exchange_copy(prefix.at[peer], incoming.at[z], p_send, p_recv, peer, z, tp).wait_send()

    @pl.loop(0, n_z)
    def _(k):
        peer = 2 * k + 1

        @pl.when(peer != me)
        def _():
            exchange_copy(state.at[k], slices.at[me], s_send, s_recv, peer, me, tp).wait_send()
            exchange_copy(own_decay.at[0], decays.at[me], e_send, e_recv, peer, me, tp).wait_send()

    for gather in (gather_x, gather_m):
        gather.drain()
    for c in (0, 1):
        for slot in range(6):
            cross(c, slot).wait_send()
        for slot in range(4):
            along(c, slot).wait_send()
        for slot in range(6):
            across(c, slot).wait_send()
    @pl.loop(1, n_ep)
    def _(d):
        peer = lax.rem(me + d, n_ep)
        exchange_copy(result.at[0], returned.at[peer], c_send, c_recv, me, peer, tp).wait_recv()

    back = returned[...].reshape(n_ep * SLOT, 128)
    eout_b[...] = (
        jnp.dot(weights[0], back, preferred_element_type=F32) + jnp.dot(weights[1], back, preferred_element_type=F32)
    ).astype(BF16)
    expert_out = pltpu.make_async_copy(eout_b, eout_hbm, out_sem.at[1])
    expert_out.start()

    mixed_out.wait()
    expert_out.wait()


def solution(mesh):
    n_ep, n_tp = mesh.shape["ep"], mesh.shape["tp"]

    def local(q, fp, v, og, floor, surge, gain, wout, rows, ngain, grp, gex, cw, wg, wu, wd):
        length, count = q.shape[0], rows.shape[0]
        hid, cols = wg.shape[2], wd.shape[2]
        n_z, exp_rows = n_ep // 2, n_ep * CAP
        half_rows = exp_rows // 2
        anyspace = pl.BlockSpec(memory_space=pl.ANY)
        dma = pltpu.SemaphoreType.DMA
        operands = (
            q, fp, v, og, floor.reshape(1, -1), surge.reshape(-1, 128), gain.reshape(1, -1), wout,
            rows, ngain.reshape(1, -1), grp.reshape(1, -1), gex.T, cw.T, wg, wu, wd.reshape(SIDE, SIDE, hid, cols),
        )
        block = (n_ep, SLOT, 128)
        part = (n_ep, 128 // n_z, 128)
        outs = (jax.ShapeDtypeStruct((length, cols), BF16), jax.ShapeDtypeStruct((count, cols), BF16))
        scratch = [pltpu.VMEM(a.shape[1:] if a.ndim == 3 else a.shape, a.dtype) for a in (*operands, *outs)]
        scratch += [
            dma((len(operands),)), dma((2,)), dma((2,)),
            pltpu.VMEM(block, BF16), pltpu.VMEM(block, BF16), pltpu.VMEM(block, BF16), pltpu.VMEM(block, BF16),
            pltpu.VMEM((2, count, n_ep * SLOT), BF16),
            pltpu.VMEM((n_z * CAP, n_z * SLOT), BF16), pltpu.VMEM((n_z * SLOT, n_z * CAP), BF16),
            pltpu.VMEM((n_tp, exp_rows, 128), BF16), pltpu.VMEM((2, SIDE, half_rows, hid), BF16),
            pltpu.VMEM((n_tp, length, 128), BF16), pltpu.VMEM((2, SIDE, SIDE, hid, cols), BF16), pltpu.VMEM((2, 2, SIDE // 2, hid, cols), BF16),
            pltpu.VMEM((2, SIDE, half_rows, cols), F32),
            pltpu.VMEM((2, 6, half_rows // 2, cols), BF16), pltpu.VMEM((2, 6, half_rows // 2, cols), BF16),
            pltpu.VMEM(q.shape, F32), pltpu.VMEM(q.shape, F32), pltpu.VMEM(q.shape, F32), pltpu.VMEM(q.shape, BF16),
            pltpu.VMEM(q.shape, F32),
            pltpu.VMEM((n_z, *part[1:]), F32), pltpu.VMEM(part, F32),
            pltpu.VMEM((n_ep, 1, 128), F32), pltpu.VMEM((1, 1, 128), F32),
            pltpu.VMEM(part, F32), pltpu.VMEM((n_z, *part[1:]), F32),
        ]
        scratch += [dma((n_ep,))] * 10 + [dma((2, 20))] * 2 + [dma((2, 4))] * 2 + [dma((2, 20))] * 2 + [dma((2, 6))] * 2 + [dma((2, 6))] * 2
        return pl.pallas_call(
            functools.partial(kernel, n_ep),
            out_shape=outs,
            in_specs=[anyspace] * len(operands),
            out_specs=(anyspace, anyspace),
            scratch_shapes=scratch,
            compiler_params=pltpu.CompilerParams(
                collective_id=0, has_side_effects=True, vmem_limit_bytes=60 * 1024 * 1024
            ),
        )(*operands)

    return jax.shard_map(
        local,
        mesh=mesh,
        in_specs=(
            P("ep", "tp"), P("ep", "tp"), P("ep", "tp"), P("ep", "tp"), P("tp"), P("ep", "tp"), P(), P(None, "tp"),
            P("ep", None), P(), P("ep"), P("ep", None), P("ep", None),
            P("ep", None, "tp"), P("ep", None, "tp"), P("ep", None, "tp"),
        ),
        out_specs=(P("ep", "tp"), P("ep", "tp")),
        check_vma=False,
    )
```

time: 101 us -> 80.2 us (0.79)
  the two profiles are of different devices: /device:TPU:2 before, /device:TPU:32 now
where the time goes in v2:
time: 80.2 us; the launch traced here: 80.1 us
  Pallas kernels  77.2 us (96%)
  local copies, waits for them, and re-layouts  2.19 us (3%)
    pallas_call x1, Pallas kernels, local(): pl.pallas_call(functools.partial(kernel, n_ep), out_shape=outs, in_specs=...  77.2 us
    unnamed x4, local copies, waits for them, and re-layouts  2.19 us

profile of v2, /device:TPU:32, one launch (start us, length us, event | category | flops | bytes accessed | tf_op | source)
XLA Modules:
  0.0 80.1 jit_solution(17642115585230598974)
XLA Ops:
  0.6 77.2 %shard_map.167 = (bf16[512,128]{1,0:T(8,128)(2,1)}, bf16[128,128]{1,0:T(8,128)(2,1)}) custom-call(bf16[512,128]{1,0:T(8,128)(2,1)} %q_hbm.1, bf16[512,128]{1,0:T(8,128)(2,1)} %fp_hbm.1, bf16[512,128]{1,0:T(8,128)(2,1)} %v_hbm.1, bf16[512,128]{1,0:T(8,128)(2,1)} %og_hbm.1, f32[1,128]{1,0:T(1,128)} %bitcast.13, f32[4,128]{1,0:T(4,128)} %bitcast.10, ...), custom_call_target="tpu_custom_call" | custom-call | tf_op jit(solution)/shard_map/pallas_call | solution.py:621
  77.9 0.0 copy-start
  77.9 1.6 %copy.20 = bf16[512,128]{1,0:T(8,128)(2,1)} copy(bf16[512,128]{1,0:T(8,128)(2,1)} %get-tuple-element.4) | data formatting | bytes 262144
  79.5 0.0 copy-done
  79.5 0.6 copy.21
Async XLA Ops:
  77.9 1.6 %copy-start = (bf16[128,128]{1,0:T(8,128)(2,1)S(1)}, bf16[128,128]{1,0:T(8,128)(2,1)}, u32[]{:S(2)}) copy-start(bf16[128,128]{1,0:T(8,128)(2,1)} %get-tuple-element.5) | copy-start | bytes 98308

commit v3 on v2

--- a/solution.py
+++ b/solution.py
@@ -12,7 +12,8 @@
 EPS = 1e-06
 GROUPS = 4
 CAP = 12
-SLOT = 16
+SUB = 4
+WIDE = CAP // SUB
 SIDE = 4
 NT = (((1,), (1,)), ((), ()))
 OFFSETS = (0, -1, 1, 2)
@@ -23,8 +24,8 @@
 
 
 class Gather:
-    def __init__(self, buf, base, rows, send, recv, ep, y, x):
-        self.buf, self.base, self.rows = buf, base, rows
+    def __init__(self, buf, leap, send, recv, ep, y, x):
+        self.buf, self.leap, self.rows = buf, leap, buf.shape[1]
         self.send, self.recv, self.ep, self.y, self.x = send, recv, ep, y, x
 
     def tp(self, color, a, b):
@@ -33,7 +34,7 @@
 
     def span(self, color, part):
         half = self.rows // 2
-        start = self.base + color * half
+        start = color * half
         if part == 1:
             return pl.ds(start, half // 2)
         if part == 2:
@@ -52,6 +53,8 @@
         )
 
     def out(self, slot):
+        if self.leap and slot == 2:
+            return (0, 0), 0, (2, 0)
         if slot < 4:
             return [((0, 0), 0, (1, 0)), ((0, 0), 0, (-1, 0)), ((-1, 0), 1, (1, 0)), ((1, 0), 2, (-1, 0))][slot]
         j, k = divmod(slot - 4, 4)
@@ -59,6 +62,8 @@
         return [((a, 0), 0, (0, 1)), ((a, 0), 0, (0, -1)), ((a, -1), 1, (0, 1)), ((a, 1), 2, (0, -1))][k]
 
     def landed(self, slot):
+        if self.leap and slot == 2:
+            return (2, 0), 0
         if slot < 4:
             return [((-1, 0), 0), ((1, 0), 0), ((2, 0), 1), ((2, 0), 2)][slot]
         j, k = divmod(slot - 4, 4)
@@ -76,7 +81,9 @@
 
     def begin(self):
         for color in (0, 1):
-            self.start(color, 0, 1, 4, 5)
+            self.start(color, *((0, 1, 2) if self.leap else (0, 1)))
+        for color in (0, 1):
+            self.start(color, 4, 5)
 
     def relay(self):
         self.relay_sends()
@@ -88,13 +95,16 @@
 
     def relay_near(self):
         self.relay_first()
+        self.opposite()
         self.relay_second()
 
     def relay_first(self):
         for k in (0, 1):
             for color in (0, 1):
                 self.arrive(color, k)
-                self.start(color, 2 + k, 4 + 4 * (k + 1), 5 + 4 * (k + 1))
+                if not self.leap:
+                    self.start(color, 2 + k)
+                self.start(color, 4 + 4 * (k + 1), 5 + 4 * (k + 1))
 
     def relay_second(self):
         for color in (0, 1):
@@ -103,10 +113,12 @@
             self.arrive(color, 5)
             self.start(color, 7)
 
+    def opposite(self):
+        for color in (0, 1):
+            self.arrive(color, *((2,) if self.leap else (2, 3)))
+            self.start(color, 16, 17)
+
     def relay_far(self):
-        for color in (0, 1):
-            self.arrive(color, 2, 3)
-            self.start(color, 16, 17)
         for j in (1, 2, 3):
             for color in (0, 1):
                 self.arrive(color, 4 + 4 * j)
@@ -122,6 +134,8 @@
     def drain(self):
         for color in (0, 1):
             for slot in range(20):
+                if self.leap and slot == 3:
+                    continue
                 self.copy(color, slot, *self.out(slot)).wait_send()
 
 
@@ -166,8 +180,8 @@
     mixed_hbm, eout_hbm,
     q_b, fp_b, v_b, og_b, floor_b, surge_b, gain_b, wout_b,
     rows_b, ngain_b, grp_b, gex_b, cw_b, wg_b, wu_b, wd_b, mixed_b, eout_b, in_sem, out_sem, own_sem,
-    outgo, arrived, result, returned, weights, pack, spread,
-    xbuf, hbuf, mbuf, wcross, staged, part, sums_out, sums_in,
+    outgo, arrived, result, returned, weights,
+    xbuf, hbuf, mbuf, wcross, staged, wide, part, sums_out, sums_in,
     cum, keyin, qact, qdec, local_out,
     state, slices, decays, own_decay, prefix, incoming,
     d_send, d_recv, c_send, c_recv,
@@ -191,17 +205,23 @@
             ("grp", grp_hbm, grp_b), ("gex", gex_hbm, gex_b), ("rows", rows_hbm, rows_b), ("ngain", ngain_hbm, ngain_b),
             ("wd", wd_hbm, wd_b), ("cw", cw_hbm, cw_b), ("floor", floor_hbm, floor_b), ("fp", fp_hbm, fp_b),
             ("surge", surge_hbm, surge_b), ("q", q_hbm, q_b), ("v", v_hbm, v_b), ("og", og_hbm, og_b),
-            ("gain", gain_hbm, gain_b), ("wg", wg_hbm.at[0], wg_b), ("wu", wu_hbm.at[0], wu_b), ("wout", wout_hbm, wout_b),
+            ("gain", gain_hbm, gain_b), ("wg", wg_hbm, wg_b), ("wu", wu_hbm, wu_b), ("wout", wout_hbm, wout_b),
         )
     ):
         loads[name] = pltpu.make_async_copy(src, dst, in_sem.at[k])
     load("grp", "gex", "rows", "ngain")
 
+    order = [(n_z // 2, c) for c in (1, 0)]
+    for away in range(n_z // 2 - 1, 0, -1):
+        order += [(way * away, c) for c in (1, 0) for way in (1, -1)]
+    order.append((0, 0))
+    peers = [lax.rem(z + away + n_z, n_z) * 2 + lax.rem(core + c + 1, 2) for away, c in order]
+
     barrier = pltpu.get_barrier_semaphore()
-    for d in range(1, n_ep):
-        pl.semaphore_signal(barrier, inc=1, device_id=(lax.rem(me + d, n_ep), tp), device_id_type=MESH)
-
-    for dy, dx in ((0, 1), (0, -1), (1, 0), (-1, 0)):
+    for peer in peers:
+        pl.semaphore_signal(barrier, inc=1, device_id=(peer, tp), device_id_type=MESH)
+
+    for dy, dx in ((0, 1), (0, -1), (1, 0), (-1, 0), (0, 2), (2, 0)):
         other = lax.rem(y + dy + SIDE, SIDE) * SIDE + lax.rem(x + dx + SIDE, SIDE)
         pl.semaphore_signal(barrier, inc=1, device_id=(me, other), device_id_type=MESH)
 
@@ -217,11 +237,13 @@
     hit0, hit1 = (e_iota == ex0).astype(F32), (e_iota == ex1).astype(F32)
     before = lax.broadcasted_iota(jnp.int32, (count, count), 0) < lax.broadcasted_iota(jnp.int32, (count, count), 1)
     earlier = jnp.dot((hit0 + hit1).astype(BF16), before.astype(F32).astype(BF16), preferred_element_type=F32)
-    slot0 = ex0 * SLOT + jnp.sum(earlier * hit0, axis=0, keepdims=True).astype(jnp.int32)
-    slot1 = ex1 * SLOT + jnp.sum(earlier * hit1, axis=0, keepdims=True).astype(jnp.int32)
-    s_iota = lax.broadcasted_iota(jnp.int32, (n_ep * SLOT, count), 0)
-    at0, at1 = s_iota == slot0, s_iota == slot1
-    place = jnp.where(at0 | at1, 1.0, 0.0).astype(BF16)
+    slot0 = ex0 * CAP + jnp.sum(earlier * hit0, axis=0, keepdims=True).astype(jnp.int32)
+    slot1 = ex1 * CAP + jnp.sum(earlier * hit1, axis=0, keepdims=True).astype(jnp.int32)
+    s_iota = lax.broadcasted_iota(jnp.int32, (n_ep * SUB, count), 0)
+    s_iota = s_iota // SUB * CAP + s_iota % SUB
+    at0 = [s_iota + q * SUB == slot0 for q in range(WIDE)]
+    at1 = [s_iota + q * SUB == slot1 for q in range(WIDE)]
+    lanes = [slice(q * 128, q * 128 + 128) for q in range(WIDE)]
 
     loads["rows"].wait()
     loads["ngain"].wait()
@@ -232,15 +254,12 @@
         square = square + piece * piece
     scale = lax.rsqrt(jnp.sum(square, axis=1, keepdims=True) * (1.0 / rows_b.shape[1]) + EPS)
     normed = (rows_b[:, columns].astype(F32) * scale * ngain_b[:, columns]).astype(BF16)
-    outgo[...] = jnp.dot(place, normed, preferred_element_type=F32).astype(BF16).reshape(outgo.shape)
-
-    pl.semaphore_wait(barrier, n_ep - 1 + 4)
-
-    order = [(n_z // 2, c) for c in (1, 0)]
-    for away in range(n_z // 2 - 1, 0, -1):
-        order += [(way * away, c) for c in (1, 0) for way in (1, -1)]
-    order.append((0, 0))
-    peers = [lax.rem(z + away + n_z, n_z) * 2 + lax.rem(core + c + 1, 2) for away, c in order]
+    for q in range(WIDE):
+        place = jnp.where(at0[q] | at1[q], 1.0, 0.0).astype(BF16)
+        block = jnp.dot(place, normed, preferred_element_type=F32).astype(BF16)
+        outgo[:, :, lanes[q]] = block.reshape(n_ep, SUB, 128)
+
+    pl.semaphore_wait(barrier, n_ep - 1 + 6)
 
     def dispatch(peer):
         return exchange_copy(outgo.at[peer], arrived.at[me], d_send, d_recv, peer, me, tp)
@@ -263,14 +282,16 @@
             there = ring_w.pos(half, off)
             return wd_b.at[there, part] if half == 0 else wd_b.at[part, there]
 
-        whole, low, high = pl.ds(0, SIDE), pl.ds(0, SIDE // 2), pl.ds(SIDE // 2, SIDE // 2)
+        low, high = pl.ds(0, SIDE // 2), pl.ds(SIDE // 2, SIDE // 2)
         src, dst = (
             (lambda: to(2, low), lambda: staged.at[half, 0]),
             (lambda: to(2, high), lambda: staged.at[half, 1]),
-            (lambda: to(1, whole), lambda: wcross.at[half, mine]),
-            (lambda: to(-1, whole), lambda: wcross.at[half, mine]),
+            (lambda: to(1, low), lambda: wcross.at[half, mine, low]),
+            (lambda: to(-1, low), lambda: wcross.at[half, mine, low]),
             (lambda: staged.at[half, 0], lambda: wcross.at[half, ring_w.pos(half, -1), low]),
             (lambda: staged.at[half, 1], lambda: wcross.at[half, ring_w.pos(half, 1), high]),
+            (lambda: to(1, high), lambda: wcross.at[half, mine, high]),
+            (lambda: to(-1, high), lambda: wcross.at[half, mine, high]),
         )[slot]
         return ring_w.copy(half, slot, src(), dst(), (1, -1)[slot % 2])
 
@@ -279,10 +300,12 @@
         region = (
             lambda: staged.at[half, 0],
             lambda: staged.at[half, 1],
-            lambda: wcross.at[half, ring_w.pos(half, -1)],
-            lambda: wcross.at[half, ring_w.pos(half, 1)],
+            lambda: wcross.at[half, ring_w.pos(half, -1), low],
+            lambda: wcross.at[half, ring_w.pos(half, 1), low],
             lambda: wcross.at[half, ring_w.pos(half, 2), low],
             lambda: wcross.at[half, ring_w.pos(half, 2), high],
+            lambda: wcross.at[half, ring_w.pos(half, -1), high],
+            lambda: wcross.at[half, ring_w.pos(half, 1), high],
         )[slot]()
         return ring_w.copy(half, slot, region, region, 1)
 
@@ -375,23 +398,17 @@
     )
     local_out[right, :] += jnp.dot(s.astype(BF16), v_b[left, :], preferred_element_type=F32)
 
-    part_rows, part_slots = n_z * CAP, n_z * SLOT
-
-    def matches(shape, axis):
-        r, s = lax.broadcasted_iota(jnp.int32, shape, axis), lax.broadcasted_iota(jnp.int32, shape, 1 - axis)
-        return jnp.where(r // CAP * SLOT + r % CAP == s, 1.0, 0.0).astype(BF16)
-
-    pack[...] = matches((part_rows, part_slots), 0)
-    spread[...] = matches((part_slots, part_rows), 1)
+    part_rows = n_z * CAP
     loads["cw"].wait()
-    chosen = jnp.where(at0, cw_b[0:1, :], 0.0) + jnp.where(at1, cw_b[1:2, :], 0.0)
-    turned = chosen.T
-    high = turned.astype(BF16)
-    weights[0] = high
-    weights[1] = (turned - high.astype(F32)).astype(BF16)
-
-    gather_x = Gather(xbuf, 0, 2 * part_rows, x_send, x_recv, me, y, x)
-    gather_m = Gather(mbuf, 0, length, m_send, m_recv, me, y, x)
+    for q in range(WIDE):
+        chosen = jnp.where(at0[q], cw_b[0:1, :], 0.0) + jnp.where(at1[q], cw_b[1:2, :], 0.0)
+        turned = chosen.T
+        high = turned.astype(BF16)
+        weights[0, :, lanes[q]] = high
+        weights[1, :, lanes[q]] = (turned - high.astype(F32)).astype(BF16)
+
+    gather_x = Gather(xbuf, True, x_send, x_recv, me, y, x)
+    gather_m = Gather(mbuf, True, m_send, m_recv, me, y, x)
     tps = SIDE * SIDE
 
     for slot in (0, 1):
@@ -405,11 +422,11 @@
         peer = lax.rem(me + d, n_ep)
         exchange_copy(outgo.at[0], arrived.at[peer], d_send, d_recv, me, peer, tp).wait_recv()
 
+    share = n_z * SUB
     for c in range(2):
-        blocks = arrived[c * n_z : (c + 1) * n_z].reshape(part_slots, 128)
-        xbuf[tp, c * part_rows : (c + 1) * part_rows, :] = jnp.dot(
-            pack[...], blocks, preferred_element_type=F32
-        ).astype(BF16)
+        for q in range(WIDE):
+            start = c * part_rows + q * share
+            xbuf[tp, start : start + share, :] = arrived[c * n_z : (c + 1) * n_z, :, lanes[q]].reshape(share, 128)
     gather_x.begin()
 
     gather_x.relay_near()
@@ -437,35 +454,46 @@
         incoming[z] = prefix[me]
 
     gather_x.relay_far()
-    gather_x.relay_last()
+    for slot in (6, 7):
+        for half in (0, 1):
+            cross(half, slot).start()
     loads["wg"].wait()
     loads["wu"].wait()
-    feats = jnp.concatenate([xbuf[k] for k in range(tps)], axis=1)
-    gate_act = jnp.dot(feats, wg_b[...], preferred_element_type=F32)
-    up_act = jnp.dot(feats, wu_b[...], preferred_element_type=F32)
-    hidden = (silu(gate_act) * up_act).astype(BF16)
-    for c in range(2):
-        hbuf[c, ring_g.pos(c)] = hidden[c * part_rows : (c + 1) * part_rows, :]
-
-    first, last = pl.ds(0, part_rows // 2), pl.ds(part_rows // 2, part_rows // 2)
+
+    def widen(c, off):
+        at = lax.rem((y, x)[c] + off + SIDE, SIDE)
+        r = slice(c * part_rows, (c + 1) * part_rows)
+        if c == 0:
+            feats = [xbuf[at * SIDE + k, r, :] for k in range(SIDE)]
+            mats = [w[at].reshape(-1, w.shape[-1]) for w in (wg_b, wu_b)]
+        else:
+            feats = [xbuf[k * SIDE + at, r, :] for k in range(SIDE)]
+            mats = [w[:, at].reshape(-1, w.shape[-1]) for w in (wg_b, wu_b)]
+        feats = jnp.concatenate(feats, axis=1)
+        return [jnp.dot(feats, w, preferred_element_type=F32) for w in mats]
+
+    for c in (0, 1):
+        pieces = [widen(c, off) for off in (0, -1, 1)]
+        for k in (0, 1):
+            wide[c, k] = pieces[0][k] + pieces[1][k] + pieces[2][k]
+    gather_x.relay_last()
+    for c in (0, 1):
+        piece = widen(c, 2)
+        hbuf[c, ring_g.pos(c)] = (silu(wide[c, 0] + piece[0]) * (wide[c, 1] + piece[1])).astype(BF16)
+
+    ways = (2, 1, -1)
 
     def along(c, slot):
-        block = hbuf.at[c, ring_g.pos(c, (0, 0, -1, 1)[slot])]
-        block = block if slot < 2 else block.at[first if slot == 2 else last]
-        return ring_g.copy(c, slot, block, block, (1, -1, 1, -1)[slot])
+        block = hbuf.at[c, ring_g.pos(c)]
+        return ring_g.copy(c, slot, block, block, ways[slot])
 
     def came_along(c, slot):
-        block = hbuf.at[c, ring_g.pos(c, (-1, 1, 2, 2)[slot])]
-        block = block if slot < 2 else block.at[first if slot == 2 else last]
-        return ring_g.copy(c, slot, block, block, 1)
-
-    for slot in (0, 1):
+        block = hbuf.at[c, ring_g.pos(c, -ways[slot])]
+        return ring_g.copy(c, slot, block, block, ways[slot])
+
+    for slot in range(3):
         for c in (0, 1):
             along(c, slot).start()
-    for slot in (0, 1):
-        for c in (0, 1):
-            came_along(c, slot).wait_recv()
-            along(c, slot + 2).start()
 
     @pl.loop(0, n_z)
     def _(k):
@@ -479,52 +507,51 @@
     out = local_out[...] + lax.dot_general(qdec[...], before_state, NT, preferred_element_type=F32)
     out = out * lax.rsqrt(jnp.mean(out * out, axis=1, keepdims=True) + EPS) * gain_b[...]
     mbuf[tp] = (out * silu(og_b[...].astype(F32))).astype(BF16)
+
     gather_m.begin()
-
     for copy in own_w:
         copy.wait()
-    for slot in (2, 3, 4, 5):
+    for slot in (2, 3, 4, 5, 6, 7):
         for c in (0, 1):
             crossed(c, slot).wait_recv()
-    for slot in (2, 3):
+
+    def narrow(c, off):
+        at = ring_g.pos(c, off)
+        feats = jnp.concatenate([wcross[c, k, at] for k in range(SIDE)], axis=1)
+        return jnp.dot(hbuf[c, at], feats, preferred_element_type=F32)
+
+    for slot in (1, 2):
         for c in (0, 1):
             came_along(c, slot).wait_recv()
-
-    sums = ((2, first, 1), (2, last, -1), (1, last, 1), (-1, first, -1), (1, first, 1), (-1, last, -1))
-
-    def across(c, slot):
-        target, rows, way = sums[slot]
-        return ring_r.copy(c, slot, sums_out.at[c, slot], sums_in.at[c, slot], way)
-
     for c in (0, 1):
-        units = jnp.concatenate([hbuf[c, k] for k in range(SIDE)], axis=1)
-        feats = jnp.concatenate([wcross[c, k].reshape(units.shape[1], 128) for k in range(SIDE)], axis=1)
-        total = jnp.dot(units, feats, preferred_element_type=F32)
+        total = narrow(c, 0) + narrow(c, -1) + narrow(c, 1)
         for k in range(SIDE):
             part[c, k] = total[:, k * 128 : (k + 1) * 128]
-        for slot in range(4):
-            target, rows, _ = sums[slot]
-            sums_out[c, slot] = part[c, ring_r.pos(c, target), rows, :].astype(BF16)
+    for c in (0, 1):
+        came_along(c, 0).wait_recv()
+
+    def across(c, slot):
+        return ring_r.copy(c, slot, sums_out.at[c, slot], sums_in.at[c, slot], ways[slot])
+
+    for c in (0, 1):
+        total = narrow(c, 2)
+        for k in range(SIDE):
+            part[c, k] += total[:, k * 128 : (k + 1) * 128]
+        for slot in range(3):
+            sums_out[c, slot] = part[c, ring_r.pos(c, ways[slot])].astype(BF16)
             across(c, slot).start()
-    for slot in (0, 1):
-        for c in (0, 1):
+    gather_m.relay_first()
+    gather_m.opposite()
+    for c in (0, 1):
+        for slot in (1, 2, 0):
             across(c, slot).wait_recv()
-            target, rows, _ = sums[slot + 4]
-            sums_out[c, slot + 4] = (
-                part[c, ring_r.pos(c, target), rows, :] + sums_in[c, slot].astype(F32)
-            ).astype(BF16)
-            across(c, slot + 4).start()
-    gather_m.relay_first()
-    for c in (0, 1):
-        for slot in (2, 3, 4, 5):
-            across(c, slot).wait_recv()
-        mine = ring_r.pos(c)
-        top = part[c, mine, first, :] + sums_in[c, 4].astype(F32) + sums_in[c, 3].astype(F32)
-        low = part[c, mine, last, :] + sums_in[c, 2].astype(F32) + sums_in[c, 5].astype(F32)
-        res = jnp.concatenate([top, low], axis=0).astype(BF16)
-        result[c * n_z : (c + 1) * n_z] = (
-            jnp.dot(spread[...], res, preferred_element_type=F32).astype(BF16).reshape(n_z, SLOT, 128)
-        )
+        res = part[c, ring_r.pos(c)]
+        for slot in range(3):
+            res = res + sums_in[c, slot].astype(F32)
+        res = res.astype(BF16)
+        for q in range(WIDE):
+            rows = res[q * share : (q + 1) * share, :]
+            result[c * n_z : (c + 1) * n_z, :, lanes[q]] = rows.reshape(n_z, SUB, 128)
 
     for peer in peers:
         give_back(peer).start()
@@ -562,18 +589,17 @@
     for gather in (gather_x, gather_m):
         gather.drain()
     for c in (0, 1):
-        for slot in range(6):
+        for slot in range(8):
             cross(c, slot).wait_send()
-        for slot in range(4):
+        for slot in range(3):
             along(c, slot).wait_send()
-        for slot in range(6):
             across(c, slot).wait_send()
     @pl.loop(1, n_ep)
     def _(d):
         peer = lax.rem(me + d, n_ep)
         exchange_copy(result.at[0], returned.at[peer], c_send, c_recv, me, peer, tp).wait_recv()
 
-    back = returned[...].reshape(n_ep * SLOT, 128)
+    back = jnp.concatenate([returned[:, :, lanes[q]].reshape(n_ep * SUB, 128) for q in range(WIDE)], axis=0)
     eout_b[...] = (
         jnp.dot(weights[0], back, preferred_element_type=F32) + jnp.dot(weights[1], back, preferred_element_type=F32)
     ).astype(BF16)
@@ -596,28 +622,29 @@
         dma = pltpu.SemaphoreType.DMA
         operands = (
             q, fp, v, og, floor.reshape(1, -1), surge.reshape(-1, 128), gain.reshape(1, -1), wout,
-            rows, ngain.reshape(1, -1), grp.reshape(1, -1), gex.T, cw.T, wg, wu, wd.reshape(SIDE, SIDE, hid, cols),
+            rows, ngain.reshape(1, -1), grp.reshape(1, -1), gex.T, cw.T,
+            wg.reshape(SIDE, SIDE, 128, hid), wu.reshape(SIDE, SIDE, 128, hid), wd.reshape(SIDE, SIDE, hid, cols),
         )
-        block = (n_ep, SLOT, 128)
+        block = (n_ep, SUB, WIDE * 128)
         part = (n_ep, 128 // n_z, 128)
         outs = (jax.ShapeDtypeStruct((length, cols), BF16), jax.ShapeDtypeStruct((count, cols), BF16))
         scratch = [pltpu.VMEM(a.shape[1:] if a.ndim == 3 else a.shape, a.dtype) for a in (*operands, *outs)]
         scratch += [
             dma((len(operands),)), dma((2,)), dma((2,)),
             pltpu.VMEM(block, BF16), pltpu.VMEM(block, BF16), pltpu.VMEM(block, BF16), pltpu.VMEM(block, BF16),
-            pltpu.VMEM((2, count, n_ep * SLOT), BF16),
-            pltpu.VMEM((n_z * CAP, n_z * SLOT), BF16), pltpu.VMEM((n_z * SLOT, n_z * CAP), BF16),
+            pltpu.VMEM((2, count, n_ep * CAP), BF16),
             pltpu.VMEM((n_tp, exp_rows, 128), BF16), pltpu.VMEM((2, SIDE, half_rows, hid), BF16),
             pltpu.VMEM((n_tp, length, 128), BF16), pltpu.VMEM((2, SIDE, SIDE, hid, cols), BF16), pltpu.VMEM((2, 2, SIDE // 2, hid, cols), BF16),
+            pltpu.VMEM((2, 2, half_rows, hid), F32),
             pltpu.VMEM((2, SIDE, half_rows, cols), F32),
-            pltpu.VMEM((2, 6, half_rows // 2, cols), BF16), pltpu.VMEM((2, 6, half_rows // 2, cols), BF16),
+            pltpu.VMEM((2, 3, half_rows, cols), BF16), pltpu.VMEM((2, 3, half_rows, cols), BF16),
             pltpu.VMEM(q.shape, F32), pltpu.VMEM(q.shape, F32), pltpu.VMEM(q.shape, F32), pltpu.VMEM(q.shape, BF16),
             pltpu.VMEM(q.shape, F32),
             pltpu.VMEM((n_z, *part[1:]), F32), pltpu.VMEM(part, F32),
             pltpu.VMEM((n_ep, 1, 128), F32), pltpu.VMEM((1, 1, 128), F32),
             pltpu.VMEM(part, F32), pltpu.VMEM((n_z, *part[1:]), F32),
         ]
-        scratch += [dma((n_ep,))] * 10 + [dma((2, 20))] * 2 + [dma((2, 4))] * 2 + [dma((2, 20))] * 2 + [dma((2, 6))] * 2 + [dma((2, 6))] * 2
+        scratch += [dma((n_ep,))] * 10 + [dma((2, 20))] * 2 + [dma((2, 3))] * 2 + [dma((2, 20))] * 2 + [dma((2, 8))] * 2 + [dma((2, 3))] * 2
         return pl.pallas_call(
             functools.partial(kernel, n_ep),
             out_shape=outs,

time: 80.2 us -> 69.6 us (0.87)
  Pallas kernels: 77.2 us -> 66.7 us
    pallas_call x1, Pallas kernels: 77.2 us -> 66.7 us  [local(): pl.pallas_call(functools.partial(kernel, n_ep), out_shape=outs, in_specs=...]
where the time goes in v3:
time: 69.6 us; the launch traced here: 69.5 us
  Pallas kernels  66.7 us (96%)
  local copies, waits for them, and re-layouts  2.19 us (3%)
    pallas_call x1, Pallas kernels, local(): pl.pallas_call(functools.partial(kernel, n_ep), out_shape=outs, in_specs=...  66.7 us
    unnamed x4, local copies, waits for them, and re-layouts  2.19 us

profile of v3, /device:TPU:32, one launch (start us, length us, event | category | flops | bytes accessed | tf_op | source)
XLA Modules:
  0.0 69.5 jit_solution(1527776328920518404)
XLA Ops:
  0.6 66.7 %shard_map.167 = (bf16[512,128]{1,0:T(8,128)(2,1)}, bf16[128,128]{1,0:T(8,128)(2,1)}) custom-call(bf16[512,128]{1,0:T(8,128)(2,1)} %q_hbm.1, bf16[512,128]{1,0:T(8,128)(2,1)} %fp_hbm.1, bf16[512,128]{1,0:T(8,128)(2,1)} %v_hbm.1, bf16[512,128]{1,0:T(8,128)(2,1)} %og_hbm.1, f32[1,128]{1,0:T(1,128)} %bitcast.17, f32[4,128]{1,0:T(4,128)} %bitcast.14, ...), custom_call_target="tpu_custom_call" | custom-call | tf_op jit(solution)/shard_map/pallas_call | solution.py:648
  67.3 0.0 copy-start
  67.3 1.6 %copy.20 = bf16[512,128]{1,0:T(8,128)(2,1)} copy(bf16[512,128]{1,0:T(8,128)(2,1)} %get-tuple-element.4) | data formatting | bytes 262144
  68.9 0.0 copy-done
  68.9 0.6 copy.21
Async XLA Ops:
  67.3 1.6 %copy-start = (bf16[128,128]{1,0:T(8,128)(2,1)S(1)}, bf16[128,128]{1,0:T(8,128)(2,1)}, u32[]{:S(2)}) copy-start(bf16[128,128]{1,0:T(8,128)(2,1)} %get-tuple-element.5) | copy-start | bytes 98308

commit v4 on v3

--- a/solution.py
+++ b/solution.py
@@ -443,12 +443,10 @@
 
         total = jnp.zeros(slices.shape[1:], F32)
         for k in range(n_ep):
-            prefix[k] = total
+            prefix[k] = total.astype(BF16)
             total = decays[k] * total + slices[k]
 
-        @pl.loop(1, n_ep)
-        def _(d):
-            peer = lax.rem(me + d, n_ep)
+        for peer in peers:
             exchange_copy(prefix.at[peer], incoming.at[z], p_send, p_recv, peer, z, tp).start()
 
         incoming[z] = prefix[me]
@@ -477,22 +475,20 @@
         for k in (0, 1):
             wide[c, k] = pieces[0][k] + pieces[1][k] + pieces[2][k]
     gather_x.relay_last()
+    ways = (2, 1, -1)
+
+    def along(c, slot):
+        block = hbuf.at[c, ring_g.pos(c)]
+        return ring_g.copy(c, slot, block, block, ways[slot])
+
+    def came_along(c, slot):
+        block = hbuf.at[c, ring_g.pos(c, -ways[slot])]
+        return ring_g.copy(c, slot, block, block, ways[slot])
+
     for c in (0, 1):
         piece = widen(c, 2)
         hbuf[c, ring_g.pos(c)] = (silu(wide[c, 0] + piece[0]) * (wide[c, 1] + piece[1])).astype(BF16)
-
-    ways = (2, 1, -1)
-
-    def along(c, slot):
-        block = hbuf.at[c, ring_g.pos(c)]
-        return ring_g.copy(c, slot, block, block, ways[slot])
-
-    def came_along(c, slot):
-        block = hbuf.at[c, ring_g.pos(c, -ways[slot])]
-        return ring_g.copy(c, slot, block, block, ways[slot])
-
-    for slot in range(3):
-        for c in (0, 1):
+        for slot in range(3):
             along(c, slot).start()
 
     @pl.loop(0, n_z)
@@ -501,7 +497,7 @@
         def _():
             exchange_copy(prefix.at[0], incoming.at[k], p_send, p_recv, me, k, tp).wait_recv()
 
-    before_state = incoming[...].reshape(128, 128).astype(BF16)
+    before_state = incoming[...].reshape(128, 128)
     loads["og"].wait()
     loads["gain"].wait()
     out = local_out[...] + lax.dot_general(qdec[...], before_state, NT, preferred_element_type=F32)
@@ -642,7 +638,7 @@
             pltpu.VMEM(q.shape, F32),
             pltpu.VMEM((n_z, *part[1:]), F32), pltpu.VMEM(part, F32),
             pltpu.VMEM((n_ep, 1, 128), F32), pltpu.VMEM((1, 1, 128), F32),
-            pltpu.VMEM(part, F32), pltpu.VMEM((n_z, *part[1:]), F32),
+            pltpu.VMEM(part, BF16), pltpu.VMEM((n_z, *part[1:]), BF16),
         ]
         scratch += [dma((n_ep,))] * 10 + [dma((2, 20))] * 2 + [dma((2, 3))] * 2 + [dma((2, 20))] * 2 + [dma((2, 8))] * 2 + [dma((2, 3))] * 2
         return pl.pallas_call(

time: 69.6 us -> 69.6 us (level)
  no operation moved by 1% of the time
where the time goes in v4:
time: 69.6 us; the launch traced here: 69.5 us
  Pallas kernels  66.7 us (96%)
  local copies, waits for them, and re-layouts  2.19 us (3%)
    pallas_call x1, Pallas kernels, local(): pl.pallas_call(functools.partial(kernel, n_ep), out_shape=outs, in_specs=...  66.7 us
    unnamed x4, local copies, waits for them, and re-layouts  2.19 us

profile of v4, /device:TPU:32, one launch (start us, length us, event | category | flops | bytes accessed | tf_op | source)
XLA Modules:
  0.0 69.5 jit_solution(7127437007946432546)
XLA Ops:
  0.6 66.7 %shard_map.167 = (bf16[512,128]{1,0:T(8,128)(2,1)}, bf16[128,128]{1,0:T(8,128)(2,1)}) custom-call(bf16[512,128]{1,0:T(8,128)(2,1)} %q_hbm.1, bf16[512,128]{1,0:T(8,128)(2,1)} %fp_hbm.1, bf16[512,128]{1,0:T(8,128)(2,1)} %v_hbm.1, bf16[512,128]{1,0:T(8,128)(2,1)} %og_hbm.1, f32[1,128]{1,0:T(1,128)} %bitcast.17, f32[4,128]{1,0:T(4,128)} %bitcast.14, ...), custom_call_target="tpu_custom_call" | custom-call | tf_op jit(solution)/shard_map/pallas_call | solution.py:644
  67.3 0.0 copy-start
  67.3 1.6 %copy.20 = bf16[512,128]{1,0:T(8,128)(2,1)} copy(bf16[512,128]{1,0:T(8,128)(2,1)} %get-tuple-element.4) | data formatting | bytes 262144
  68.9 0.0 copy-done
  68.9 0.6 copy.21
Async XLA Ops:
  67.3 1.6 %copy-start = (bf16[128,128]{1,0:T(8,128)(2,1)S(1)}, bf16[128,128]{1,0:T(8,128)(2,1)}, u32[]{:S(2)}) copy-start(bf16[128,128]{1,0:T(8,128)(2,1)} %get-tuple-element.5) | copy-start | bytes 98308
